TPU v7x, 32 devices: a whole 2x2x4 slice. The times are simulated.
32 devices in a mesh: sp: 16 (over z, y, core), tp: 2 (over x).
Axes of the slice: x: 2, y: 2, z: 4, core: 2. Of those that a mesh axis runs over, the one named last changes fastest.
Arguments:
- tokens_in: bfloat16 [4096, 2048], P('sp', 'tp'), may hold values from -400 to 400
- norm_gain: float32 [2048], replicated, may hold values from 0.1 to 1.9
- w_query: bfloat16 [2048, 1024], P('sp', 'tp'), may hold values from -0.125 to 0.125
- w_forget: bfloat16 [2048, 1024], P('sp', 'tp'), may hold values from -0.125 to 0.125
- w_input: bfloat16 [2048, 1024], P('sp', 'tp'), may hold values from -0.125 to 0.125
- w_rgate: bfloat16 [2048, 1024], P('sp', 'tp'), may hold values from -0.125 to 0.125
- w_pool_in: bfloat16 [2048, 1024], P('sp', 'tp'), may hold values from -0.125 to 0.125
- w_pgate: bfloat16 [2048, 1024], P('sp', 'tp'), may hold values from -0.125 to 0.125
- floor_rate: float32 [1024], P('tp'), as said below
- extra_logdecay: float32 [4096, 8], P('sp', 'tp'), as said below
- state_gain: float32 [1024], P('tp'), may hold values from 0.1 to 1.9
- pool_mix: bfloat16 [8, 128, 128], P('tp'), may hold values from -0.5 to 0.5
- pool_gain: float32 [1024], P('tp'), may hold values from 0.1 to 1.9
- out_rec: bfloat16 [1024, 2048], P('tp', 'sp'), may hold values from -0.125 to 0.125
- out_pool: bfloat16 [1024, 2048], P('tp', 'sp'), may hold values from -0.125 to 0.125
- post_gain: float32 [2048], replicated, may hold values from 0.1 to 1.9
Outputs:
- mixed_out: bfloat16 [4096, 2048], P(('sp', 'tp'))
Inputs may be any that keep to these rules, and one draw needn't show every extreme that they name: `floor_rate`: every entry is positive. `extra_logdecay`: every entry is at most zero.
All inputs are finite; a program needn't handle non-finite values.
Results may differ from a plain program's by a relative error of at most 0.015.
Values may be sent and summed in bfloat16 or wider, within the bound.
A program may use at most 64 MiB of HBM per device.

v0:
```python
import functools

import jax
import jax.numpy as jnp
from jax import lax
from jax.experimental import pallas as pl
from jax.experimental.pallas import tpu as pltpu
from jax.sharding import PartitionSpec as P

DK = 128


eps = 1e-06
coarsest_scale_depth = lax.Precision.HIGHEST


PIECES = 4


def ring_place(chip, chips):
    odd = chip % 2
    return (1 - odd) * (chip // 2) + odd * (chips - 1 - chip // 2)


def ring_chip(place, chips):
    back = place // (chips // 2)
    return (1 - back) * (2 * place) + back * (2 * (chips - 1 - place) + 1)


def project_kernel(
    n,
    n_tp,
    tok_ref,
    gain_ref,
    w0,
    w1,
    w2,
    w3,
    w4,
    w5,
    proj_ref,
    wide,
    scaled,
    weights,
    acc,
    tok_send,
    tok_recv,
    own_sem,
    ring_send,
    ring_recv,
    core_send,
    core_recv,
):
    chips = n // 2
    steps = chips // 2
    me = lax.axis_index("sp")
    tp = lax.axis_index("tp")
    core = me % 2
    place = ring_place(me // 2, chips)

    def chip_at(offset):
        return ring_chip((place + offset + chips) % chips, chips)

    following = 2 * chip_at(1) + core
    preceding = 2 * chip_at(-1) + core
    partner = 2 * (me // 2) + 1 - core
    parts = (w0, w1, w2, w3, w4, w5)
    rows, part_cols = w0.shape
    my_rows = pl.ds(pl.multiple_of(me * rows, 16), rows)
    owns = []
    for i, part in enumerate(parts):
        block = weights.at[my_rows, pl.ds(i * part_cols, part_cols)]
        owns.append(pltpu.make_async_copy(part, block, own_sem.at[i]))
        owns[-1].start()
    piece = rows // PIECES
    features = tok_ref.shape[1]

    barrier = pltpu.get_barrier_semaphore()
    for peer in (following, preceding, partner):
        pl.semaphore_signal(barrier, inc=1, device_id={"sp": peer})
    for turn in range(1, n_tp):
        pl.semaphore_signal(barrier, inc=1, device_id={"tp": (tp + turn) % n_tp})
    pl.semaphore_wait(barrier, 3 + n_tp - 1)

    def rows_of(chip, which, q):
        start = (2 * chip + which) * rows + q * piece
        return pl.ds(pl.multiple_of(start, 8), piece)

    sends = []

    def to_core(offset, q, source):
        slot = offset + steps - 1
        copy = pltpu.make_async_remote_copy(
            src_ref=source,
            dst_ref=weights.at[rows_of(chip_at(offset), core, q)],
            send_sem=core_send.at[slot, q],
            recv_sem=core_recv.at[slot, q],
            device_id={"sp": partner},
        )
        copy.start()
        sends.append(copy)

    def from_core(offset, q):
        slot = offset + steps - 1
        dst = weights.at[rows_of(chip_at(offset), 1 - core, q)]
        pltpu.make_async_remote_copy(
            src_ref=dst,
            dst_ref=dst,
            send_sem=core_send.at[slot, q],
            recv_sem=core_recv.at[slot, q],
            device_id={"sp": partner},
        ).wait_recv()

    def pieces_of(direction, step):
        if step < steps - 1:
            return range(PIECES)
        half = PIECES // 2
        return range(half) if direction == 0 else range(half, PIECES)

    def ring_copy(direction, step, q, source):
        offset = -step if direction == 0 else step
        dst = weights.at[rows_of(chip_at(offset), core, q)]
        return pltpu.make_async_remote_copy(
            src_ref=dst if source is None else source,
            dst_ref=dst,
            send_sem=ring_send.at[direction, step, q],
            recv_sem=ring_recv.at[direction, step, q],
            device_id={"sp": following if direction == 0 else preceding},
        )

    def ring_arrival(direction, step, q):
        offset = -(step + 1) if direction == 0 else step + 1
        dst = weights.at[rows_of(chip_at(offset), core, q)]
        pltpu.make_async_remote_copy(
            src_ref=dst,
            dst_ref=dst,
            send_sem=ring_send.at[direction, step, q],
            recv_sem=ring_recv.at[direction, step, q],
            device_id={"sp": following if direction == 0 else preceding},
        ).wait_recv()

    for own in owns:
        own.wait()
    for q in range(PIECES):
        mine = weights.at[rows_of(me // 2, core, q)]
        for direction in range(2):
            if q in pieces_of(direction, 0):
                copy = ring_copy(direction, 0, q, mine)
                copy.start()
                sends.append(copy)
        to_core(0, q, mine)
    tokens_at = pl.ds(pl.multiple_of(tp * features, 128), features)
    for turn in range(1, n_tp):
        copy = pltpu.make_async_remote_copy(
            src_ref=tok_ref,
            dst_ref=wide.at[:, tokens_at],
            send_sem=tok_send.at[turn - 1],
            recv_sem=tok_recv.at[turn - 1],
            device_id={"tp": (tp + turn) % n_tp},
        )
        copy.start()
        sends.append(copy)
    acc[...] = jnp.zeros_like(acc)
    wide[:, tokens_at] = tok_ref[...]
    for turn in range(1, n_tp):
        theirs = pl.ds(
            pl.multiple_of((tp - turn + n_tp) % n_tp * features, 128), features
        )
        pltpu.make_async_remote_copy(
            src_ref=tok_ref,
            dst_ref=wide.at[:, theirs],
            send_sem=tok_send.at[turn - 1],
            recv_sem=tok_recv.at[turn - 1],
            device_id={"tp": (tp + turn) % n_tp},
        ).wait_recv()
    scaled[...] = (wide[...].astype(jnp.float32) * gain_ref[...]).astype(jnp.bfloat16)

    cols = weights.shape[1]
    tile = cols // 6

    by_chip = (2 * rows) % 128 == 0

    def multiply(offset):
        if not by_chip:
            return
        multiply_rows(pl.ds(pl.multiple_of(chip_at(offset) * 2 * rows, 2 * rows), 2 * rows))

    def multiply_rows(depth):
        def one(i, _):
            at = pl.ds(pl.multiple_of(i * tile, 128), tile)
            acc[:, at] += jnp.dot(
                scaled[:, depth], weights[depth, at], preferred_element_type=jnp.float32
            )
            return 0

        lax.fori_loop(0, 6, one, 0)

    for step in range(steps):
        for q in range(PIECES):
            for direction in range(2):
                if q not in pieces_of(direction, step):
                    continue
                offset = -(step + 1) if direction == 0 else step + 1
                ring_arrival(direction, step, q)
                if step + 1 < steps and q in pieces_of(direction, step + 1):
                    copy = ring_copy(direction, step + 1, q, None)
                    copy.start()
                    sends.append(copy)
                last = offset if abs(offset) < steps else steps
                dst = weights.at[rows_of(chip_at(last), core, q)]
                to_core(last, q, dst)
        for offset in [0] if step == 0 else [-step, step]:
            for q in range(PIECES):
                from_core(offset, q)
            multiply(offset)
    for q in range(PIECES):
        from_core(steps, q)
    multiply(steps)
    if not by_chip:
        multiply_rows(slice(None))
    values = wide[...].astype(jnp.float32)
    squares = jnp.sum(values * values, axis=1, keepdims=True)
    inv_rms = lax.rsqrt(squares / wide.shape[1] + eps)
    proj_ref[...] = (acc[...] * inv_rms).astype(jnp.bfloat16)
    for copy in sends:
        copy.wait_send()


def project(tokens, gain, shards):
    n = lax.axis_size("sp")
    n_tp = lax.axis_size("tp")
    positions, features = tokens.shape
    rows = shards[0].shape[0]
    cols = sum(shard.shape[1] for shard in shards)
    width = n * rows
    steps = n // 4
    dma = pltpu.SemaphoreType.DMA
    return pl.pallas_call(
        functools.partial(project_kernel, n, n_tp),
        out_shape=jax.ShapeDtypeStruct((positions, cols), jnp.bfloat16),
        in_specs=[pl.BlockSpec(memory_space=pltpu.VMEM)] * 2
        + [pl.BlockSpec(memory_space=pl.ANY)] * 6,
        out_specs=pl.BlockSpec(memory_space=pltpu.VMEM),
        scratch_shapes=[
            pltpu.VMEM((positions, width), jnp.bfloat16),
            pltpu.VMEM((positions, width), jnp.bfloat16),
            pltpu.VMEM((width, cols), jnp.bfloat16),
            pltpu.VMEM((positions, cols), jnp.float32),
            dma((n_tp,)),
            dma((n_tp,)),
            dma((6,)),
            dma((2, steps, PIECES)),
            dma((2, steps, PIECES)),
            dma((2 * steps, PIECES)),
            dma((2 * steps, PIECES)),
        ],
        compiler_params=pltpu.CompilerParams(
            collective_id=0, has_side_effects=True, vmem_limit_bytes=56 * 1024 * 1024
        ),
        cost_estimate=pl.CostEstimate(
            flops=2 * positions * width * cols, bytes_accessed=4 * rows * cols, transcendentals=0
        ),
    )(tokens, gain[None, :], *shards)


def mix_kernel(
    n,
    n_tp,
    proj_ref,
    keep_ref,
    extra_ref,
    sgain_ref,
    mix_ref,
    pgain_ref,
    w_ref,
    post_ref,
    out_ref,
    weights,
    local,
    reach,
    both,
    state,
    before,
    gone_state,
    gone_decay,
    come_state,
    come_decay,
    tail,
    tail_in,
    mine,
    gone_out,
    come_out,
    ring_send,
    ring_recv,
    core_send,
    core_recv,
    scan_send,
    scan_recv,
    tail_sem,
    own_sem,
    out_send,
    out_recv,
):
    f32, bf16 = jnp.float32, jnp.bfloat16
    chips = n // 2
    steps = chips // 2
    rounds = (n - 1).bit_length()
    me = lax.axis_index("sp")
    tp = lax.axis_index("tp")
    core = me % 2
    place = ring_place(me // 2, chips)

    def chip_at(offset):
        return ring_chip((place + offset + chips) % chips, chips)

    following = 2 * chip_at(1) + core
    preceding = 2 * chip_at(-1) + core
    partner = 2 * (me // 2) + 1 - core
    piece = w_ref.shape[0] // PIECES

    barrier = pltpu.get_barrier_semaphore()
    for peer in (following, preceding, partner):
        pl.semaphore_signal(barrier, inc=1, device_id={"sp": peer})
    for r in range(rounds):
        pl.semaphore_signal(barrier, inc=1, device_id={"sp": (me + 2**r) % n})
        pl.semaphore_signal(barrier, inc=1, device_id={"sp": (me - 2**r + n) % n})
    for turn in range(1, n_tp):
        pl.semaphore_signal(barrier, inc=1, device_id={"tp": (tp + turn) % n_tp})
    pl.semaphore_wait(barrier, 3 + 2 * rounds + n_tp - 1)

    sends = []

    def spot(chip, which, q):
        return weights.at[2 * chip + which, pl.ds(q * piece, piece)]

    def to_core(offset, q, source):
        slot = offset + steps - 1
        copy = pltpu.make_async_remote_copy(
            src_ref=source,
            dst_ref=spot(chip_at(offset), core, q),
            send_sem=core_send.at[slot, q],
            recv_sem=core_recv.at[slot, q],
            device_id={"sp": partner},
        )
        copy.start()
        sends.append(copy)

    def from_core(offset, q):
        slot = offset + steps - 1
        dst = spot(chip_at(offset), 1 - core, q)
        pltpu.make_async_remote_copy(
            src_ref=dst,
            dst_ref=dst,
            send_sem=core_send.at[slot, q],
            recv_sem=core_recv.at[slot, q],
            device_id={"sp": partner},
        ).wait_recv()

    def pieces_of(direction, step):
        if step < steps - 1:
            return range(PIECES)
        half = PIECES // 2
        return range(half) if direction == 0 else range(half, PIECES)

    def ring_copy(direction, step, q, source, offset):
        dst = spot(chip_at(offset), core, q)
        return pltpu.make_async_remote_copy(
            src_ref=dst if source is None else source,
            dst_ref=dst,
            send_sem=ring_send.at[direction, step, q],
            recv_sem=ring_recv.at[direction, step, q],
            device_id={"sp": following if direction == 0 else preceding},
        )

    def ring_step(step):
        for q in range(PIECES):
            for direction in range(2):
                if q not in pieces_of(direction, step):
                    continue
                offset = -(step + 1) if direction == 0 else step + 1
                ring_copy(direction, step, q, None, offset).wait_recv()
                if step + 1 < steps and q in pieces_of(direction, step + 1):
                    copy = ring_copy(direction, step + 1, q, None, offset)
                    copy.start()
                    sends.append(copy)
                last = offset if abs(offset) < steps else steps
                to_core(last, q, spot(chip_at(last), core, q))

    pending = list(range(steps))

    def advance_ring():
        if pending:
            ring_step(pending.pop(0))

    positions = proj_ref.shape[0]
    head_cols = proj_ref.shape[1] // 6
    heads = head_cols // DK
    reach_back = tail.shape[0]

    tail[...] = proj_ref[positions - reach_back :, 4 * head_cols : 5 * head_cols]
    for q in range(PIECES):
        own_piece = w_ref.at[pl.ds(q * piece, piece)]
        for direction in range(2):
            if q in pieces_of(direction, 0):
                copy = ring_copy(direction, 0, q, own_piece, 0)
                copy.start()
                sends.append(copy)
        to_core(0, q, own_piece)
    own = pltpu.make_async_copy(w_ref, weights.at[me], own_sem)
    own.start()
    tail_copy = pltpu.make_async_remote_copy(
        src_ref=tail,
        dst_ref=tail_in,
        send_sem=tail_sem.at[0],
        recv_sem=tail_sem.at[1],
        device_id={"sp": (me + 1) % n},
    )
    tail_copy.start()

    row = lax.broadcasted_iota(jnp.int32, (positions, positions), 0)
    col = lax.broadcasted_iota(jnp.int32, (positions, positions), 1)
    lower = jnp.where(row >= col, 1.0, 0.0).astype(f32)
    line = lax.broadcasted_iota(jnp.int32, (positions, DK), 0)
    units = positions // 8
    sub = lax.broadcasted_iota(jnp.int32, (units, 8, DK), 1)
    over_last = (((1,), (1,)), ((), ()))

    decay_now = []
    for h in range(heads):
        at = slice(h * DK, (h + 1) * DK)
        part = lambda i: proj_ref[:, i * head_cols + h * DK : i * head_cols + (h + 1) * DK]
        q = part(0).astype(f32) * DK ** (-0.5)
        kg = keep_ref[:, at] * jax.nn.sigmoid(-part(1).astype(f32))
        v = part(2)
        logs = jnp.log1p(-kg) + extra_ref[:, h : h + 1]
        c = jnp.dot(
            lower, logs, precision=coarsest_scale_depth, preferred_element_type=f32
        )
        last = c[positions - 1 :, :]
        state[h] = lax.dot_general(
            v,
            (kg * jnp.exp(last - c)).astype(bf16),
            (((0,), (0,)), ((), ())),
            preferred_element_type=f32,
        )
        gone_decay[0, h : h + 1, :] = jnp.exp(last)
        reach[:, at] = (q * jnp.exp(c)).astype(bf16)
        scores = jnp.zeros((positions, positions), f32)
        span = 8
        while span < positions:
            pair = 2 * span
            c3 = c.reshape(positions // pair, pair, DK)
            middle = jnp.broadcast_to(c3[:, span - 1 : span, :], c3.shape).reshape(c.shape)
            fade = jnp.exp(-jnp.abs(c - middle))
            later = (line // span) % 2 == 1
            probe = jnp.where(later, q * fade, 0.0).astype(bf16)
            keyed = jnp.where(later, 0.0, kg * fade).astype(bf16)
            found = lax.dot_general(probe, keyed, over_last, preferred_element_type=f32)
            scores = scores + jnp.where(row // pair == col // pair, found, 0.0)
            span = pair
        result = jnp.dot(scores.astype(bf16), v, preferred_element_type=f32)
        c3 = c.reshape(units, 8, DK)
        q3 = q.reshape(units, 8, DK)
        k3 = kg.reshape(units, 8, DK)
        v3 = v.astype(f32).reshape(units, 8, DK)
        near = result.reshape(units, 8, DK)
        for s in range(8):
            weight = jnp.exp(jnp.minimum(c3 - c3[:, s : s + 1, :], 0.0))
            score = jnp.sum(q3 * k3[:, s : s + 1, :] * weight, axis=2, keepdims=True)
            near = near + jnp.where(sub >= s, score * v3[:, s : s + 1, :], 0.0)
        local[:, at] = near.reshape(positions, DK)
        if h % 2 == 1:
            advance_ring()

    def scan_copies(r):
        target = {"sp": (me + 2**r) % n}
        return [
            pltpu.make_async_remote_copy(
                src_ref=gone.at[r],
                dst_ref=come.at[r],
                send_sem=scan_send.at[r, i],
                recv_sem=scan_recv.at[r, i],
                device_id=target,
            )
            for i, (gone, come) in enumerate(
                [(gone_state, come_state), (gone_decay, come_decay)]
            )
        ]

    before[...] = jnp.zeros_like(before)
    decay_w = [gone_decay[0, h : h + 1, :] for h in range(heads)]
    decay_e = [jnp.ones((1, DK), f32) for h in range(heads)]

    def pool(h):
        at = slice(h * DK, (h + 1) * DK)
        x = proj_ref[:, 4 * head_cols + h * DK : 4 * head_cols + (h + 1) * DK].astype(f32)
        prior = jnp.where(me > 0, tail_in[:, at].astype(f32), 0.0)
        level = (tp * heads + h) % 4
        total = jnp.concatenate([prior, x], axis=0)
        chosen = jnp.zeros((positions, DK), f32)
        for k in range(4):
            total = total + pltpu.roll(total, 2**k, 0)
            chosen = jnp.where(level == k, total[reach_back:, :], chosen)
        window = 2
        for k in range(1, 4):
            window = jnp.where(level == k, 2 ** (1 + k), window)
        count = jnp.minimum(me * positions + line + 1, window).astype(f32)
        mixed = (chosen / count - x).astype(bf16)
        mapped = jnp.dot(mixed, mix_ref[h], preferred_element_type=f32)
        gate = proj_ref[:, 5 * head_cols + h * DK : 5 * head_cols + (h + 1) * DK].astype(f32)
        both[:, head_cols + h * DK : head_cols + (h + 1) * DK] = (
            mapped * pgain_ref[:, at] * (gate * jax.nn.sigmoid(gate))
        ).astype(bf16)

    pools = list(range(heads))
    for r in range(rounds):
        gone_state[r] = state[...].astype(bf16)
        if r > 0:
            for h in range(heads):
                gone_decay[r, h : h + 1, :] = decay_w[h]
        for copy in scan_copies(r):
            copy.start()
            sends.append(copy)
        if r == 0:
            tail_copy.wait_recv()
        if pools:
            pool(pools.pop(0))
        advance_ring()
        for copy in scan_copies(r):
            copy.wait_recv()
        valid = me >= 2**r
        for h in range(heads):
            came = jnp.where(valid, come_state[r, h].astype(f32), 0.0)
            came_decay = jnp.where(valid, come_decay[r, h : h + 1, :], 1.0)
            before[h] = before[h] + decay_e[h] * came
            decay_e[h] = decay_e[h] * came_decay
            if r + 1 < rounds:
                state[h] = state[h] + decay_w[h] * came
                decay_w[h] = decay_w[h] * came_decay
    for h in pools:
        pool(h)
    while pending:
        advance_ring()

    for h in range(heads):
        at = slice(h * DK, (h + 1) * DK)
        rec = local[:, at] + lax.dot_general(
            reach[:, at], before[h].astype(bf16), over_last, preferred_element_type=f32
        )
        normed = rec * lax.rsqrt(jnp.mean(rec * rec, axis=1, keepdims=True) + eps)
        gate = proj_ref[:, 3 * head_cols + h * DK : 3 * head_cols + (h + 1) * DK].astype(f32)
        both[:, at] = (normed * sgain_ref[:, at] * (gate * jax.nn.sigmoid(gate))).astype(bf16)

    own.wait()
    for offset in range(-(steps - 1), steps + 1):
        for q in range(PIECES):
            from_core(offset, q)

    owned = positions // n_tp
    width = w_ref.shape[1]
    quarter = n // 4

    def share(rows, group):
        left = both[rows, :]
        for slot in range(group * quarter, (group + 1) * quarter, 2):
            right = jnp.concatenate([weights[slot], weights[slot + 1]], axis=1)
            yield slot, jnp.dot(left, right, preferred_element_type=f32).astype(bf16)

    def out_copy(turn, group):
        cols = pl.ds(group * quarter * width, quarter * width)
        return pltpu.make_async_remote_copy(
            src_ref=gone_out.at[turn - 1, :, cols],
            dst_ref=come_out.at[turn - 1, :, cols],
            send_sem=out_send.at[turn - 1, group],
            recv_sem=out_recv.at[turn - 1, group],
            device_id={"tp": (tp + turn) % n_tp},
        )

    for turn in range(1, n_tp):
        target = (tp + turn) % n_tp
        rows = pl.ds(pl.multiple_of(target * owned, owned), owned)
        for group in range(4):
            for slot, value in share(rows, group):
                gone_out[turn - 1, :, slot * width : (slot + 2) * width] = value
            copy = out_copy(turn, group)
            copy.start()
            sends.append(copy)
    rows = pl.ds(pl.multiple_of(tp * owned, owned), owned)
    for group in range(4):
        for slot, value in share(rows, group):
            mine[:, slot * width : (slot + 2) * width] = value.astype(f32)
    for turn in range(1, n_tp):
        for group in range(4):
            out_copy(turn, group).wait_recv()
        mine[...] += come_out[turn - 1].astype(f32)
    summed = mine[...]
    out_ref[...] = (
        summed
        * lax.rsqrt(jnp.mean(summed * summed, axis=1, keepdims=True) + eps)
        * post_ref[...]
    ).astype(bf16)
    tail_copy.wait_send()
    for copy in sends:
        copy.wait_send()


def mix(proj, keep, extra, sgain, pool_mix, pgain, shard, post):
    n = lax.axis_size("sp")
    n_tp = lax.axis_size("tp")
    positions, heads = extra.shape
    head_cols = heads * DK
    depth, width = shard.shape
    steps = n // 4
    rounds = (n - 1).bit_length()
    owned = positions // n_tp
    model = n * width
    padded = -(-heads // 8) * 8
    f32, bf16, dma = jnp.float32, jnp.bfloat16, pltpu.SemaphoreType.DMA
    return pl.pallas_call(
        functools.partial(mix_kernel, n, n_tp),
        out_shape=jax.ShapeDtypeStruct((owned, model), bf16),
        in_specs=[pl.BlockSpec(memory_space=pltpu.VMEM)] * 8,
        out_specs=pl.BlockSpec(memory_space=pltpu.VMEM),
        scratch_shapes=[
            pltpu.VMEM((n, depth, width), bf16),
            pltpu.VMEM((positions, head_cols), f32),
            pltpu.VMEM((positions, head_cols), bf16),
            pltpu.VMEM((positions, 2 * head_cols), bf16),
            pltpu.VMEM((heads, DK, DK), f32),
            pltpu.VMEM((heads, DK, DK), f32),
            pltpu.VMEM((rounds, heads, DK, DK), bf16),
            pltpu.VMEM((rounds, padded, DK), f32),
            pltpu.VMEM((rounds, heads, DK, DK), bf16),
            pltpu.VMEM((rounds, padded, DK), f32),
            pltpu.VMEM((16, head_cols), bf16),
            pltpu.VMEM((16, head_cols), bf16),
            pltpu.VMEM((owned, model), f32),
            pltpu.VMEM((n_tp, owned, model), bf16),
            pltpu.VMEM((n_tp, owned, model), bf16),
            dma((2, steps, PIECES)),
            dma((2, steps, PIECES)),
            dma((2 * steps, PIECES)),
            dma((2 * steps, PIECES)),
            dma((rounds, 2)),
            dma((rounds, 2)),
            dma((2,)),
            dma,
            dma((n_tp, 4)),
            dma((n_tp, 4)),
        ],
        compiler_params=pltpu.CompilerParams(
            collective_id=1, has_side_effects=True, vmem_limit_bytes=56 * 1024 * 1024
        ),
        cost_estimate=pl.CostEstimate(
            flops=2 * positions * depth * model, bytes_accessed=4 * depth * width, transcendentals=0
        ),
    )(proj, keep, extra, sgain, pool_mix, pgain, shard, post)


def per_device(
    tokens_in,
    norm_gain,
    w_query,
    w_forget,
    w_input,
    w_rgate,
    w_pool_in,
    w_pgate,
    floor_rate,
    extra_logdecay,
    state_gain,
    pool_mix,
    pool_gain,
    out_rec,
    out_pool,
    post_gain,
):
    shards = [w_query, w_forget, w_input, w_rgate, w_pool_in, w_pgate]
    proj = project(tokens_in, norm_gain, shards)
    return mix(
        proj,
        -jnp.expm1(-floor_rate)[None, :],
        extra_logdecay,
        state_gain[None, :],
        pool_mix,
        pool_gain[None, :],
        jnp.concatenate([out_rec, out_pool], axis=0),
        post_gain[None, :],
    )


def solution(mesh):
    placed = (
        P("sp", "tp"),
        P(),
        P("sp", "tp"),
        P("sp", "tp"),
        P("sp", "tp"),
        P("sp", "tp"),
        P("sp", "tp"),
        P("sp", "tp"),
        P("tp"),
        P("sp", "tp"),
        P("tp"),
        P("tp", None, None),
        P("tp"),
        P("tp", "sp"),
        P("tp", "sp"),
        P(),
    )
    return jax.shard_map(
        per_device, mesh=mesh, in_specs=placed, out_specs=P(("sp", "tp"), None), check_vma=False
    )
```

profile of v0, /device:TPU:0, one launch (start us, length us, event | category | flops | bytes accessed | tf_op | source)
XLA Modules:
  0.0 138.2 jit_solution(15646827555638565104)
XLA Ops:
  0.0 1.3 exponential-minus-one_negate_fusion
  1.3 1.5 %copy.17.extra_ref = f32[256,4]{1,0:T(8,128)} copy(f32[256,4]{0,1:T(4,128)} %param.25) | data formatting | bytes 8192 | tf_op args[9]
  2.8 1.7 %pad_maximum_fusion.w_ref = bf16[1024,128]{1,0:T(8,128)(2,1)} fusion(bf16[512,128]{1,0:T(8,128)(2,1)} %param.30, bf16[512,128]{1,0:T(8,128)(2,1)} %param.29), kind=kLoop, calls=%fused_computation | loop fusion | flops 524288 | bytes 524288 | tf_op jit(solution)/shard_map/concatenate | solution.py:687
  4.5 72.3 %shard_map.154.proj_ref = bf16[256,3072]{1,0:T(8,128)(2,1)} custom-call(bf16[256,1024]{1,0:T(8,128)(2,1)} %tok_ref.1, f32[1,2048]{1,0:T(1,128)} %bitcast.6, bf16[128,512]{1,0:T(8,128)(2,1)} %w0.1, bf16[128,512]{1,0:T(8,128)(2,1)} %w1.1, bf16[128,512]{1,0:T(8,128)(2,1)} %w2.1, bf16[128,512]{1,0:T(8,128)(2,1)} %w3.1, bf16[128,512]{1,0:T(8,128)(2,1)} %w4.1, ...), custom_call_target="tpu_custom_call" | custom-call | flops 3221225472 | bytes 1572864 | tf_op jit(solution)/shard_map/pallas_call | solution.py:238
  76.8 59.6 %shard_map.155 = bf16[128,2048]{1,0:T(8,128)(2,1)} custom-call(bf16[256,3072]{1,0:T(8,128)(2,1)} %shard_map.154.proj_ref, f32[1,512]{1,0:T(1,128)} %bitcast.5, f32[256,4]{1,0:T(8,128)} %copy.17.extra_ref, f32[1,512]{1,0:T(1,128)} %bitcast.8, bf16[4,128,128]{2,1,0:T(8,128)(2,1)} %mix_ref.1, f32[1,512]{1,0:T(1,128)} %bitcast.9, ...), custom_call_target="tpu_custom_call" | custom-call | flops 1073741824 | bytes 524288 | tf_op jit(solution)/shard_map/pallas_call | solution.py:619
  136.3 1.9 %copy.19 = bf16[128,2048]{1,0:T(8,128)(2,1)} copy(bf16[128,2048]{1,0:T(8,128)(2,1)} %shard_map.155) | data formatting | bytes 1048576
where the time goes:
time: 138 us
  Pallas kernels  132 us (96%)
  local copies, waits for them, and re-layouts  3.36 us (2%)
  other arithmetic  2.97 us (2%)
    pallas_call x1, Pallas kernels, project(): pl.pallas_call(functools.partial(project_kernel, n, n_tp), out_shape=jax....  72.3 us
    pallas_call x1, Pallas kernels, mix(): pl.pallas_call(functools.partial(mix_kernel, n, n_tp), out_shape=jax.Shap...  59.6 us
    unnamed x2, local copies, waits for them, and re-layouts  3.36 us

commit v1 on v0

--- a/solution.py
+++ b/solution.py
@@ -657,6 +657,670 @@
     )(proj, keep, extra, sgain, pool_mix, pgain, shard, post)
 
 
+def pair_kernel(
+    tok_hbm,
+    gain_ref,
+    w0,
+    w1,
+    w2,
+    w3,
+    w4,
+    w5,
+    rate_ref,
+    extra_hbm,
+    sgain_ref,
+    mix_hbm,
+    pgain_ref,
+    orec_hbm,
+    opool_hbm,
+    post_ref,
+    out_ref,
+    wide,
+    scaled,
+    inv_rms,
+    w_own,
+    w_all,
+    o_all,
+    extra,
+    mix_own,
+    proj,
+    local,
+    reach,
+    state,
+    state_go,
+    state_come,
+    decay_go,
+    decay_come,
+    tail_go,
+    tail_come,
+    total_go,
+    total_come,
+    last_go,
+    last_come,
+    y_all,
+    y_go,
+    part_go,
+    part_come,
+    mine,
+    own_sem,
+    tok_send,
+    tok_recv,
+    extra_send,
+    extra_recv,
+    w_send,
+    w_recv,
+    wy_send,
+    wy_recv,
+    o_send,
+    o_recv,
+    oy_send,
+    oy_recv,
+    scan_send,
+    scan_recv,
+    y_send,
+    y_recv,
+    part_send,
+    part_recv,
+):
+    f32, bf16 = jnp.float32, jnp.bfloat16
+    me = lax.axis_index("sp")
+    x = lax.axis_index("tp")
+    z, y, c = me // 4, (me // 2) % 2, me % 2
+    odd = z % 2
+    pair = z // 2
+    head = odd * 2 + c
+    slabs = [z, z + 1 - 2 * odd, (z + 2) % 4, 3 - z]
+    rows, feats = tok_hbm.shape
+    shard = w0.shape[0]
+    parts = (w0, w1, w2, w3, w4, w5)
+    units = len(parts)
+    positions = wide.shape[0]
+    half = positions // 2
+    block = rows
+    blocks = positions // block
+    piece = rows // 2
+
+    def peer(zz, yy, cc):
+        return {"sp": zz * 4 + yy * 2 + cc}
+
+    def peer_x(cc):
+        return {"sp": z * 4 + y * 2 + cc, "tp": 1 - x}
+
+    other_c = peer(z, y, 1 - c)
+    other_y = peer(z, 1 - y, c)
+
+    def lanes(i, n=1):
+        return pl.ds(pl.multiple_of(i * DK, DK), n * DK)
+
+    def own_rows(base, size):
+        return pl.ds(pl.multiple_of(base, 16), size)
+
+    def tok_at(zq, cc, xx, q):
+        start = zq * half + cc * rows + q * piece
+        return wide.at[own_rows(start, piece), pl.ds(pl.multiple_of(xx * feats, 128), feats)]
+
+    owns = {}
+
+    def own_copy(name, src, dst):
+        copy = pltpu.make_async_copy(src, dst, own_sem.at[len(owns)])
+        copy.start()
+        owns[name] = copy
+
+    for q in range(2):
+        own_copy(("tok", q), tok_hbm.at[pl.ds(q * piece, piece)], tok_at(odd, c, x, q))
+    for u, part in enumerate(parts):
+        own_copy(("w", u), part, w_own.at[u])
+    own_copy("extra", extra_hbm, extra.at[odd * 2 + c])
+    here = z * 2 + y
+    own_copy(("o", 0), orec_hbm, o_all.at[here, pl.ds(0, 4 * DK)])
+    own_copy(("o", 1), opool_hbm, o_all.at[here, pl.ds(4 * DK, 4 * DK)])
+    own_copy("mix", mix_hbm.at[head], mix_own)
+
+    barrier = pltpu.get_barrier_semaphore()
+    peers = [other_c, other_y, peer_x(c), peer_x(1 - c)]
+    for k in range(1, 4):
+        peers += [peer(slabs[k], y, c), peer(slabs[k], y, 1 - c)]
+    for to in peers:
+        pl.semaphore_signal(barrier, inc=1, device_id=to)
+    pl.semaphore_wait(barrier, len(peers))
+
+    sends = []
+
+    def send(src, dst, send_sem, recv_sem, to):
+        copy = pltpu.make_async_remote_copy(
+            src_ref=src, dst_ref=dst, send_sem=send_sem, recv_sem=recv_sem, device_id=to
+        )
+        copy.start()
+        sends.append(copy)
+
+    def arrive(dst, send_sem, recv_sem, to):
+        pltpu.make_async_remote_copy(
+            src_ref=dst, dst_ref=dst, send_sem=send_sem, recv_sem=recv_sem, device_id=to
+        ).wait_recv()
+
+    def tok_send_to(kind, q, zq, cc, xx, to):
+        at = tok_at(zq, cc, xx, q)
+        send(at, at, tok_send.at[kind, q], tok_recv.at[kind, q], to)
+
+    def tok_arrive(kind, q, zq, cc, xx):
+        at = tok_at(zq, cc, xx, q)
+        arrive(at, tok_send.at[kind, q], tok_recv.at[kind, q], other_c)
+
+    for q in range(2):
+        owns[("tok", q)].wait()
+        tok_send_to(0, q, odd, c, x, peer(slabs[1], y, c))
+        tok_send_to(1, q, odd, c, x, peer_x(c))
+        tok_send_to(3, q, odd, c, x, other_c)
+
+    def w_piece(slab, cc, n=1):
+        return own_rows((slab * 4 + y * 2 + cc) * shard, n * shard)
+
+    w_locals = []
+    for u in range(units):
+        owns[("w", u)].wait()
+        keep_here = pltpu.make_async_copy(
+            w_own.at[u, :, lanes(head)], w_all.at[u, w_piece(z, c)], own_sem.at[len(owns) + u]
+        )
+        keep_here.start()
+        w_locals.append(keep_here)
+        send(
+            w_own.at[u, :, lanes(odd * 2 + 1 - c)],
+            w_all.at[u, w_piece(z, c)],
+            w_send.at[u, 0, 1],
+            w_recv.at[u, 0, 1],
+            other_c,
+        )
+        for k in (1, 2, 3):
+            for e in range(2):
+                cc = c if e == 0 else 1 - c
+                to_head = (slabs[k] % 2) * 2 + cc
+                send(
+                    w_own.at[u, :, lanes(to_head)],
+                    w_all.at[u, w_piece(z, c)],
+                    w_send.at[u, k, e],
+                    w_recv.at[u, k, e],
+                    peer(slabs[k], y, cc),
+                )
+    owns["extra"].wait()
+    for e, to in enumerate([other_c, peer(slabs[1], y, c), peer(slabs[1], y, 1 - c)]):
+        at = extra.at[odd * 2 + c]
+        send(at, at, extra_send.at[e], extra_recv.at[e], to)
+
+    def w_relay(u, k):
+        if k == 0:
+            w_locals[u].wait()
+        else:
+            arrive(
+                w_all.at[u, w_piece(slabs[k], c)], w_send.at[u, k, 0], w_recv.at[u, k, 0], other_c
+            )
+        arrive(
+            w_all.at[u, w_piece(slabs[k], 1 - c)], w_send.at[u, k, 1], w_recv.at[u, k, 1], other_c
+        )
+        at = w_all.at[u, w_piece(slabs[k], 0, 2)]
+        send(at, at, wy_send.at[u, k], wy_recv.at[u, k], other_y)
+
+    def w_need(u):
+        for k in range(4):
+            start = (slabs[k] * 4 + (1 - y) * 2) * shard
+            at = w_all.at[u, own_rows(start, 2 * shard)]
+            arrive(at, wy_send.at[u, k], wy_recv.at[u, k], other_y)
+
+    def o_at(slab, yy, part):
+        return o_all.at[slab * 2 + yy, pl.ds(part * 4 * DK, 4 * DK)]
+
+    def o_out(part):
+        for k in (1, 2, 3):
+            at = o_at(z, y, part)
+            send(at, at, o_send.at[k, part], o_recv.at[k, part], peer(slabs[k], y, c))
+
+    def o_relay(k, part):
+        at = o_at(slabs[k], y, part)
+        if k > 0:
+            arrive(at, o_send.at[k, part], o_recv.at[k, part], other_c)
+        send(at, at, oy_send.at[k, part], oy_recv.at[k, part], other_y)
+
+    def o_need(k):
+        for part in range(2):
+            at = o_at(slabs[k], 1 - y, part)
+            arrive(at, oy_send.at[k, part], oy_recv.at[k, part], other_y)
+
+    for u in range(units):
+        w_relay(u, 0)
+    for part in range(2):
+        owns[("o", part)].wait()
+    o_out(0)
+
+    def tok_z(q):
+        tok_arrive(0, q, 1 - odd, c, x)
+        tok_send_to(2, q, 1 - odd, c, x, peer_x(c))
+        tok_send_to(4, q, 1 - odd, c, x, other_c)
+
+    def tok_x(q):
+        tok_arrive(1, q, odd, c, 1 - x)
+        tok_send_to(5, q, odd, c, 1 - x, other_c)
+
+    def tok_diagonal(q):
+        tok_arrive(2, q, 1 - odd, c, 1 - x)
+        tok_send_to(6, q, 1 - odd, c, 1 - x, other_c)
+
+    def scale(zq, cc):
+        at = own_rows(zq * half + cc * rows, rows)
+        values = wide[at, :].astype(f32)
+        scaled[at, :] = (values * gain_ref[...]).astype(bf16)
+        squares = jnp.sum(values * values, axis=1, keepdims=True)
+        inv_rms[at, :] = jnp.broadcast_to(
+            lax.rsqrt(squares / wide.shape[1] + eps), (rows, DK)
+        )
+
+    todo = []
+
+    def plan(tag, fn, *args):
+        todo.append((tag, lambda: fn(*args)))
+
+    def pump(count=1):
+        for _ in range(count):
+            if todo:
+                todo.pop(0)[1]()
+
+    def upto(tag):
+        while any(t == tag for t, _ in todo):
+            pump()
+
+    plan("t", tok_z, 0)
+    plan("w0", w_relay, 0, 2)
+    plan("w0", w_relay, 0, 3)
+    plan("t", tok_z, 1)
+    plan("tx", tok_x, 0)
+    plan("tx", tok_x, 1)
+    plan("w0", w_relay, 0, 1)
+    for k in (2, 3, 1):
+        plan("w1", w_relay, 1, k)
+    plan("td", tok_diagonal, 0)
+    plan("w2", w_relay, 2, 2)
+    plan("w2", w_relay, 2, 3)
+    plan("td", tok_diagonal, 1)
+    plan("w2", w_relay, 2, 1)
+    for u in range(3, units):
+        for k in (2, 3, 1):
+            plan("w%d" % u, w_relay, u, k)
+    for k in (2, 3, 1):
+        plan("o", o_relay, k, 0)
+
+    upto("tx")
+    o_relay(0, 0)
+    o_relay(0, 1)
+    scale(odd, c)
+    for q in range(2):
+        tok_arrive(3, q, odd, 1 - c, x)
+        tok_arrive(5, q, odd, 1 - c, 1 - x)
+    scale(odd, 1 - c)
+    upto("td")
+    scale(1 - odd, c)
+    for q in range(2):
+        tok_arrive(4, q, 1 - odd, 1 - c, x)
+        tok_arrive(6, q, 1 - odd, 1 - c, 1 - x)
+    scale(1 - odd, 1 - c)
+
+    def project_units(first, count):
+        def one(i, _):
+            at = own_rows(i * block, block)
+            right = [w_all[u] for u in range(first, first + count)]
+            right = right[0] if count == 1 else jnp.concatenate(right, axis=1)
+            acc = jnp.dot(scaled[at, :], right, preferred_element_type=f32)
+            norm = inv_rms[at, :]
+            for j in range(count):
+                proj[first + j, at, :] = (acc[:, j * DK : (j + 1) * DK] * norm).astype(bf16)
+            return 0
+
+        lax.fori_loop(0, blocks, one, 0)
+
+    upto("w1")
+    w_need(0)
+    w_need(1)
+    project_units(0, 2)
+    for e, (zq, cc) in enumerate([(odd, 1 - c), (1 - odd, c), (1 - odd, 1 - c)]):
+        arrive(extra.at[zq * 2 + cc], extra_send.at[e], extra_recv.at[e], other_c)
+    upto("w2")
+    w_need(2)
+    project_units(2, 1)
+
+    rate = rate_ref[:, lanes(head)]
+    series = jnp.ones_like(rate)
+    for n in range(10, 1, -1):
+        series = 1.0 - series * rate / n
+    keep = jnp.where(rate < 0.5, rate * series, 1.0 - jnp.exp(-rate))
+
+    row = lax.broadcasted_iota(jnp.int32, (block, block), 0)
+    col = lax.broadcasted_iota(jnp.int32, (block, block), 1)
+    lower = jnp.where(row >= col, 1.0, 0.0).astype(f32)
+    line = lax.broadcasted_iota(jnp.int32, (block, DK), 0)
+    eighths = block // 8
+    sub = lax.broadcasted_iota(jnp.int32, (eighths, 8, DK), 1)
+    over_last = (((1,), (1,)), ((), ()))
+    decays = []
+    for b in range(blocks):
+        at = slice(b * block, (b + 1) * block)
+        q = proj[1, at, :].astype(f32) * DK ** (-0.5)
+        kg = keep * jax.nn.sigmoid(-proj[0, at, :].astype(f32))
+        v = proj[2, at, :]
+        added = jnp.broadcast_to(extra[b, pl.ds(head, 1), :], (DK, block)).T
+        logs = jnp.log1p(-kg) + added
+        cum = jnp.dot(lower, logs, precision=coarsest_scale_depth, preferred_element_type=f32)
+        last = cum[block - 1 :, :]
+        state[b] = lax.dot_general(
+            v,
+            (kg * jnp.exp(last - cum)).astype(bf16),
+            (((0,), (0,)), ((), ())),
+            preferred_element_type=f32,
+        )
+        decays.append(jnp.exp(last))
+        reach[at, :] = (q * jnp.exp(cum)).astype(bf16)
+        scores = jnp.zeros((block, block), f32)
+        span = 8
+        while span < block:
+            twice = 2 * span
+            c3 = cum.reshape(block // twice, twice, DK)
+            middle = jnp.broadcast_to(c3[:, span - 1 : span, :], c3.shape).reshape(cum.shape)
+            fade = jnp.exp(-jnp.abs(cum - middle))
+            later = (line // span) % 2 == 1
+            probe = jnp.where(later, q * fade, 0.0).astype(bf16)
+            keyed = jnp.where(later, 0.0, kg * fade).astype(bf16)
+            found = lax.dot_general(probe, keyed, over_last, preferred_element_type=f32)
+            scores = scores + jnp.where(row // twice == col // twice, found, 0.0)
+            span = twice
+        result = jnp.dot(scores.astype(bf16), v, preferred_element_type=f32)
+        c3 = cum.reshape(eighths, 8, DK)
+        q3 = q.reshape(eighths, 8, DK)
+        k3 = kg.reshape(eighths, 8, DK)
+        v3 = v.astype(f32).reshape(eighths, 8, DK)
+        near = result.reshape(eighths, 8, DK)
+        for s in range(8):
+            weight = jnp.exp(jnp.minimum(c3 - c3[:, s : s + 1, :], 0.0))
+            score = jnp.sum(q3 * k3[:, s : s + 1, :] * weight, axis=2, keepdims=True)
+            near = near + jnp.where(sub >= s, score * v3[:, s : s + 1, :], 0.0)
+        local[at, :] = near.reshape(block, DK)
+        if b == 0:
+            upto("w3")
+        elif b == 1:
+            pump(1)
+        else:
+            pump(1)
+
+    sums = [decays[2 * i + 1] * state[2 * i] + state[2 * i + 1] for i in range(2)]
+    fades = [decays[2 * i] * decays[2 * i + 1] for i in range(2)]
+    for i in range(2):
+        state_go[i] = sums[i].astype(bf16)
+        decay_go[i : i + 1, :] = fades[i]
+    send(state_go, state_come, scan_send.at[0], scan_recv.at[0], other_y)
+    send(decay_go, decay_come, scan_send.at[1], scan_recv.at[1], other_y)
+    w_need(3)
+    project_units(3, 1)
+    for i in range(2):
+        tail_go[i] = proj[3, (i + 1) * half - 16 : (i + 1) * half, :]
+    send(tail_go, tail_come, scan_send.at[2], scan_recv.at[2], other_y)
+    upto("w4")
+
+    arrive(state_come, scan_send.at[0], scan_recv.at[0], other_y)
+    arrive(decay_come, scan_send.at[1], scan_recv.at[1], other_y)
+    first_y = y == 0
+    theirs = [state_come[i].astype(f32) for i in range(2)]
+    their_fades = [decay_come[i : i + 1, :] for i in range(2)]
+    order = []
+    for i in range(2):
+        order.append(
+            (jnp.where(first_y, sums[i], theirs[i]), jnp.where(first_y, fades[i], their_fades[i]))
+        )
+        order.append(
+            (jnp.where(first_y, theirs[i], sums[i]), jnp.where(first_y, their_fades[i], fades[i]))
+        )
+    total = order[0][0]
+    for add, fade in order[1:]:
+        total = fade * total + add
+    total_go[...] = total.astype(bf16)
+    arrive(tail_come, scan_send.at[2], scan_recv.at[2], other_y)
+    last_go[...] = jnp.where(first_y, tail_come[1].astype(f32), tail_go[1].astype(f32)).astype(bf16)
+    across = peer(slabs[2], y, c)
+    send(total_go, total_come, scan_send.at[3], scan_recv.at[3], across)
+    send(last_go, last_come, scan_send.at[4], scan_recv.at[4], across)
+
+    upto("w5")
+    w_need(4)
+    w_need(5)
+    project_units(4, 2)
+    owns["mix"].wait()
+    arrive(total_come, scan_send.at[3], scan_recv.at[3], across)
+    arrive(last_come, scan_send.at[4], scan_recv.at[4], across)
+
+    later_pair = pair > 0
+    at_head = lanes(head)
+    level = (x * 4 + head) % 4
+    window = 2
+    for k in range(1, 4):
+        window = jnp.where(level == k, 2 ** (1 + k), window)
+    line_half = lax.broadcasted_iota(jnp.int32, (half, DK), 0)
+    far = [jnp.where(later_pair, last_come[...].astype(f32), 0.0), tail_come[0].astype(f32)]
+    their_tails = [tail_come[i].astype(f32) for i in range(2)]
+    befores = []
+    running = jnp.where(later_pair, total_come[...].astype(f32), 0.0)
+    for i in range(2):
+        after_first = order[2 * i][1] * running + order[2 * i][0]
+        befores.append(jnp.where(first_y, running, after_first))
+        running = order[2 * i + 1][1] * after_first + order[2 * i + 1][0]
+
+    def y_half(i):
+        at = own_rows(i * half, half)
+        at_static = slice(i * half, (i + 1) * half)
+        xin = proj[3, at_static, :].astype(f32)
+        prior = jnp.where(first_y, far[i], their_tails[i])
+        sums_in = jnp.concatenate([prior, xin], axis=0)
+        chosen = jnp.zeros((half, DK), f32)
+        for k in range(4):
+            sums_in = sums_in + pltpu.roll(sums_in, 2**k, 0)
+            chosen = jnp.where(level == k, sums_in[16:, :], chosen)
+        begins = (4 * pair + 2 * i + y) * half
+        count = jnp.minimum(begins + line_half + 1, window).astype(f32)
+        mixed = (chosen / count - xin).astype(bf16)
+        mapped = jnp.dot(mixed, mix_own[...], preferred_element_type=f32)
+        gate = proj[5, at_static, :].astype(f32)
+        pooled = (mapped * pgain_ref[:, at_head] * (gate * jax.nn.sigmoid(gate))).astype(bf16)
+        cur = befores[i]
+        recs = []
+        for j in range(2):
+            b = 2 * i + j
+            rows_b = slice(b * block, (b + 1) * block)
+            rec = local[rows_b, :] + lax.dot_general(
+                reach[rows_b, :], cur.astype(bf16), over_last, preferred_element_type=f32
+            )
+            cur = decays[b] * cur + state[b]
+            normed = rec * lax.rsqrt(jnp.mean(rec * rec, axis=1, keepdims=True) + eps)
+            gate = proj[4, rows_b, :].astype(f32)
+            recs.append(
+                (normed * sgain_ref[:, at_head] * (gate * jax.nn.sigmoid(gate))).astype(bf16)
+            )
+        return jnp.concatenate(recs, axis=0), pooled
+
+    halves = [y_half(i) for i in range(2)]
+    is_odd = odd == 1
+    for part in range(2):
+        low, high = halves[0][part].astype(f32), halves[1][part].astype(f32)
+        y_go[part] = jnp.where(is_odd, low, high).astype(bf16)
+        y_all[part * 4 + head] = jnp.where(is_odd, high, low).astype(bf16)
+    z_peer = peer(slabs[1], y, c)
+    their_head = (1 - odd) * 2 + c
+    for part in range(2):
+        send(
+            y_go.at[part],
+            y_all.at[part * 4 + head],
+            y_send.at[0, part],
+            y_recv.at[0, part],
+            z_peer,
+        )
+        at = y_all.at[part * 4 + head]
+        send(at, at, y_send.at[1, part], y_recv.at[1, part], other_c)
+    o_out(1)
+    upto("o")
+    for part in range(2):
+        at = y_all.at[part * 4 + their_head]
+        arrive(at, y_send.at[0, part], y_recv.at[0, part], z_peer)
+        send(at, at, y_send.at[2, part], y_recv.at[2, part], other_c)
+    for part in range(2):
+        at = y_all.at[part * 4 + odd * 2 + 1 - c]
+        arrive(at, y_send.at[1, part], y_recv.at[1, part], other_c)
+    for part in range(2):
+        at = y_all.at[part * 4 + (1 - odd) * 2 + 1 - c]
+        arrive(at, y_send.at[2, part], y_recv.at[2, part], other_c)
+
+    owned = part_come.shape[2]
+    part_peers = [(x, 1 - c, other_c), (1 - x, c, peer_x(c)), (1 - x, 1 - c, peer_x(1 - c))]
+
+    def rows_for(xx, cc):
+        return own_rows(cc * rows + xx * owned, owned)
+
+    def out_chunk(k):
+        if k > 0:
+            o_relay(k, 1)
+        o_need(k)
+        left = jnp.concatenate([y_all[i] for i in range(8)], axis=1)
+        right = jnp.concatenate([o_all[slabs[k] * 2], o_all[slabs[k] * 2 + 1]], axis=1)
+        part_go[k] = jnp.dot(left, right, preferred_element_type=f32).astype(bf16)
+        for i, (xx, cc, to) in enumerate(part_peers):
+            send(
+                part_go.at[k, rows_for(xx, cc)],
+                part_come.at[k, i],
+                part_send.at[k, i],
+                part_recv.at[k, i],
+                to,
+            )
+
+    def gather_chunk(k):
+        for i, (xx, cc, to) in enumerate(part_peers):
+            arrive(part_come.at[k, i], part_send.at[k, i], part_recv.at[k, i], to)
+        ours = part_go[k, rows_for(x, c), :].astype(f32) + part_come[k, 1].astype(f32)
+        others = part_come[k, 0].astype(f32) + part_come[k, 2].astype(f32)
+        for yy in range(2):
+            cols = slice(yy * DK, (yy + 1) * DK)
+            mine[:, lanes(slabs[k] * 4 + yy * 2 + c)] = ours[:, cols]
+            mine[:, lanes(slabs[k] * 4 + yy * 2 + 1 - c)] = others[:, cols]
+
+    turns = (0, 2, 3, 1)
+    for turn, k in enumerate(turns):
+        out_chunk(k)
+        if turn > 0:
+            gather_chunk(turns[turn - 1])
+    gather_chunk(turns[-1])
+    summed = mine[...]
+    out_ref[...] = (
+        summed
+        * lax.rsqrt(jnp.mean(summed * summed, axis=1, keepdims=True) + eps)
+        * post_ref[...]
+    ).astype(bf16)
+    for copy in sends:
+        copy.wait_send()
+
+
+def pair_layer(
+    tokens,
+    gain,
+    shards,
+    rate,
+    extra,
+    sgain,
+    pool_mix,
+    pgain,
+    out_rec,
+    out_pool,
+    post,
+):
+    n = lax.axis_size("sp")
+    n_tp = lax.axis_size("tp")
+    rows, feats = tokens.shape
+    shard, cols = shards[0].shape
+    heads = cols // DK
+    depth, width = out_rec.shape
+    slabs = n // 4
+    positions = 4 * rows
+    half = 2 * rows
+    owned = rows // n_tp
+    model = n * width
+    f32, bf16, dma = jnp.float32, jnp.bfloat16, pltpu.SemaphoreType.DMA
+    units = len(shards)
+    vmem, hbm = pl.BlockSpec(memory_space=pltpu.VMEM), pl.BlockSpec(memory_space=pl.ANY)
+    return pl.pallas_call(
+        pair_kernel,
+        out_shape=jax.ShapeDtypeStruct((owned, model), bf16),
+        in_specs=[hbm, vmem] + [hbm] * 6 + [vmem, hbm, vmem, hbm, vmem, hbm, hbm, vmem],
+        out_specs=vmem,
+        scratch_shapes=[
+            pltpu.VMEM((positions, n_tp * feats), bf16),
+            pltpu.VMEM((positions, n_tp * feats), bf16),
+            pltpu.VMEM((positions, DK), f32),
+            pltpu.VMEM((units, shard, cols), bf16),
+            pltpu.VMEM((units, n * shard, DK), bf16),
+            pltpu.VMEM((2 * slabs, 2 * depth, width), bf16),
+            pltpu.VMEM((4, heads, rows), f32),
+            pltpu.VMEM((DK, DK), bf16),
+            pltpu.VMEM((units, positions, DK), bf16),
+            pltpu.VMEM((positions, DK), f32),
+            pltpu.VMEM((positions, DK), bf16),
+            pltpu.VMEM((4, DK, DK), f32),
+            pltpu.VMEM((2, DK, DK), bf16),
+            pltpu.VMEM((2, DK, DK), bf16),
+            pltpu.VMEM((8, DK), f32),
+            pltpu.VMEM((8, DK), f32),
+            pltpu.VMEM((2, 16, DK), bf16),
+            pltpu.VMEM((2, 16, DK), bf16),
+            pltpu.VMEM((DK, DK), bf16),
+            pltpu.VMEM((DK, DK), bf16),
+            pltpu.VMEM((16, DK), bf16),
+            pltpu.VMEM((16, DK), bf16),
+            pltpu.VMEM((2 * heads, half, DK), bf16),
+            pltpu.VMEM((2, half, DK), bf16),
+            pltpu.VMEM((slabs, half, 2 * width), bf16),
+            pltpu.VMEM((slabs, 3, owned, 2 * width), bf16),
+            pltpu.VMEM((owned, model), f32),
+            dma((2 * units + 6,)),
+            dma((7, 2)),
+            dma((7, 2)),
+            dma((3,)),
+            dma((3,)),
+            dma((units, slabs, 2)),
+            dma((units, slabs, 2)),
+            dma((units, slabs)),
+            dma((units, slabs)),
+            dma((slabs, 2)),
+            dma((slabs, 2)),
+            dma((slabs, 2)),
+            dma((slabs, 2)),
+            dma((5,)),
+            dma((5,)),
+            dma((3, 2)),
+            dma((3, 2)),
+            dma((slabs, 3)),
+            dma((slabs, 3)),
+        ],
+        compiler_params=pltpu.CompilerParams(
+            collective_id=0, has_side_effects=True, vmem_limit_bytes=56 * 1024 * 1024
+        ),
+        cost_estimate=pl.CostEstimate(
+            flops=2 * positions * n * shard * units * DK,
+            bytes_accessed=4 * units * shard * cols,
+            transcendentals=0,
+        ),
+    )(
+        tokens,
+        gain[None, :],
+        *shards,
+        rate[None, :],
+        extra.T,
+        sgain[None, :],
+        pool_mix,
+        pgain[None, :],
+        out_rec,
+        out_pool,
+        post[None, :],
+    )
+
+
 def per_device(
     tokens_in,
     norm_gain,
@@ -675,6 +1339,21 @@
     out_pool,
     post_gain,
 ):
+    n, n_tp, heads = lax.axis_size("sp"), lax.axis_size("tp"), extra_logdecay.shape[1]
+    if n == 16 and n_tp == 2 and heads == 4:
+        return pair_layer(
+            tokens_in,
+            norm_gain,
+            [w_forget, w_query, w_input, w_pool_in, w_rgate, w_pgate],
+            floor_rate,
+            extra_logdecay,
+            state_gain,
+            pool_mix,
+            pool_gain,
+            out_rec,
+            out_pool,
+            post_gain,
+        )
     shards = [w_query, w_forget, w_input, w_rgate, w_pool_in, w_pgate]
     proj = project(tokens_in, norm_gain, shards)
     return mix(

time: 138 us -> 111 us (0.80)
  the two profiles are of different devices: /device:TPU:0 before, /device:TPU:9 now
where the time goes in v1:
time: 111 us
  Pallas kernels  109 us (98%)
  local copies, waits for them, and re-layouts  1.88 us (2%)
    pallas_call x1, Pallas kernels, pair_layer(): pl.pallas_call(pair_kernel, out_shape=jax.ShapeDtypeStruct((owned, model)...  109 us

profile of v1, /device:TPU:9, one launch (start us, length us, event | category | flops | bytes accessed | tf_op | source)
XLA Modules:
  0.0 110.5 jit_solution(5593371442489540965)
XLA Ops:
  0.0 108.6 %shard_map.154 = bf16[128,2048]{1,0:T(8,128)(2,1)} custom-call(bf16[256,1024]{1,0:T(8,128)(2,1)} %tok_hbm.1, f32[1,2048]{1,0:T(1,128)} %bitcast.6, bf16[128,512]{1,0:T(8,128)(2,1)} %w0.1, bf16[128,512]{1,0:T(8,128)(2,1)} %w1.1, bf16[128,512]{1,0:T(8,128)(2,1)} %w2.1, bf16[128,512]{1,0:T(8,128)(2,1)} %w3.1, bf16[128,512]{1,0:T(8,128)(2,1)} %w4.1, ...), custom_call_target="tpu_custom_call" | custom-call | flops 3221225472 | bytes 1572864 | tf_op jit(solution)/shard_map/pallas_call | solution.py:1248
  108.6 1.9 %copy.18 = bf16[128,2048]{1,0:T(8,128)(2,1)} copy(bf16[128,2048]{1,0:T(8,128)(2,1)} %shard_map.154) | data formatting | bytes 1048576

commit v2 on v1

--- a/solution.py
+++ b/solution.py
@@ -686,6 +686,9 @@
     proj,
     local,
     reach,
+    faded,
+    kept,
+    scored,
     state,
     state_go,
     state_come,
@@ -729,7 +732,9 @@
     odd = z % 2
     pair = z // 2
     head = odd * 2 + c
-    slabs = [z, z + 1 - 2 * odd, (z + 2) % 4, 3 - z]
+    is_mid = (z == 1) | (z == 2)
+    slabs = [z, z + 1 - 2 * odd, 2 - pair, 3 * (1 - pair)]
+    my_slot = jnp.where(is_mid, 2, 3)
     rows, feats = tok_hbm.shape
     shard = w0.shape[0]
     parts = (w0, w1, w2, w3, w4, w5)
@@ -815,6 +820,41 @@
     def w_piece(slab, cc, n=1):
         return own_rows((slab * 4 + y * 2 + cc) * shard, n * shard)
 
+    def send_copy(src, dst, send_sem, recv_sem, to):
+        return pltpu.make_async_remote_copy(
+            src_ref=src, dst_ref=dst, send_sem=send_sem, recv_sem=recv_sem, device_id=to
+        )
+
+    def w_send_to(u, k, only=None):
+        copies = []
+        for e in range(2):
+            cc = c if e == 0 else 1 - c
+            slot = 1 if k == 1 else my_slot
+            copies.append(
+                send_copy(
+                    w_own.at[u, :, lanes((slabs[k] % 2) * 2 + cc)],
+                    w_all.at[u, w_piece(z, c)],
+                    w_send.at[u, k, e],
+                    w_recv.at[u, slot, e],
+                    peer(slabs[k], y, cc),
+                )
+            )
+        issue(copies, only, last=only is not is_mid)
+
+    def issue(copies, only=None, last=True):
+        if only is None:
+            for copy in copies:
+                copy.start()
+        else:
+
+            @pl.when(only)
+            def _():
+                for copy in copies:
+                    copy.start()
+
+        if last:
+            sends.extend(copies)
+
     w_locals = []
     for u in range(units):
         owns[("w", u)].wait()
@@ -830,17 +870,9 @@
             w_recv.at[u, 0, 1],
             other_c,
         )
-        for k in (1, 2, 3):
-            for e in range(2):
-                cc = c if e == 0 else 1 - c
-                to_head = (slabs[k] % 2) * 2 + cc
-                send(
-                    w_own.at[u, :, lanes(to_head)],
-                    w_all.at[u, w_piece(z, c)],
-                    w_send.at[u, k, e],
-                    w_recv.at[u, k, e],
-                    peer(slabs[k], y, cc),
-                )
+        w_send_to(u, 1)
+    for u in range(units):
+        w_send_to(u, 2, is_mid)
     owns["extra"].wait()
     for e, to in enumerate([other_c, peer(slabs[1], y, c), peer(slabs[1], y, 1 - c)]):
         at = extra.at[odd * 2 + c]
@@ -857,7 +889,23 @@
             w_all.at[u, w_piece(slabs[k], 1 - c)], w_send.at[u, k, 1], w_recv.at[u, k, 1], other_c
         )
         at = w_all.at[u, w_piece(slabs[k], 0, 2)]
-        send(at, at, wy_send.at[u, k], wy_recv.at[u, k], other_y)
+        send_copy(at, at, wy_send.at[u, k], wy_recv.at[u, k], other_y).start()
+
+    def w_relay_mid():
+        @pl.when(is_mid)
+        def _():
+            for u in range(units):
+                w_relay(u, 2)
+
+    def w_relay_end(u):
+        @pl.when(jnp.logical_not(is_mid))
+        def _():
+            w_relay(u, 2)
+
+    def w_late():
+        for u in range(units):
+            w_send_to(u, 2, jnp.logical_not(is_mid))
+            w_send_to(u, 3)
 
     def w_need(u):
         for k in range(4):
@@ -865,13 +913,23 @@
             at = w_all.at[u, own_rows(start, 2 * shard)]
             arrive(at, wy_send.at[u, k], wy_recv.at[u, k], other_y)
 
+    pieces = 4
+    depth = o_all.shape[1] // pieces
+
     def o_at(slab, yy, part):
-        return o_all.at[slab * 2 + yy, pl.ds(part * 4 * DK, 4 * DK)]
-
-    def o_out(part):
-        for k in (1, 2, 3):
+        return o_all.at[slab * 2 + yy, pl.ds(part * depth, depth)]
+
+    def o_out(k, only=None, which=range(pieces)):
+        slot = 1 if k == 1 else my_slot
+        copies = []
+        for part in which:
             at = o_at(z, y, part)
-            send(at, at, o_send.at[k, part], o_recv.at[k, part], peer(slabs[k], y, c))
+            copies.append(
+                send_copy(
+                    at, at, o_send.at[k, part], o_recv.at[slot, part], peer(slabs[k], y, c)
+                )
+            )
+        issue(copies, only, last=only is not is_mid)
 
     def o_relay(k, part):
         at = o_at(slabs[k], y, part)
@@ -880,15 +938,16 @@
         send(at, at, oy_send.at[k, part], oy_recv.at[k, part], other_y)
 
     def o_need(k):
-        for part in range(2):
+        for part in range(pieces):
             at = o_at(slabs[k], 1 - y, part)
             arrive(at, oy_send.at[k, part], oy_recv.at[k, part], other_y)
+
+    is_end = jnp.logical_not(is_mid)
 
     for u in range(units):
         w_relay(u, 0)
     for part in range(2):
         owns[("o", part)].wait()
-    o_out(0)
 
     def tok_z(q):
         tok_arrive(0, q, 1 - odd, c, x)
@@ -912,54 +971,35 @@
             lax.rsqrt(squares / wide.shape[1] + eps), (rows, DK)
         )
 
-    todo = []
-
-    def plan(tag, fn, *args):
-        todo.append((tag, lambda: fn(*args)))
-
-    def pump(count=1):
-        for _ in range(count):
-            if todo:
-                todo.pop(0)[1]()
-
-    def upto(tag):
-        while any(t == tag for t, _ in todo):
-            pump()
-
-    plan("t", tok_z, 0)
-    plan("w0", w_relay, 0, 2)
-    plan("w0", w_relay, 0, 3)
-    plan("t", tok_z, 1)
-    plan("tx", tok_x, 0)
-    plan("tx", tok_x, 1)
-    plan("w0", w_relay, 0, 1)
-    for k in (2, 3, 1):
-        plan("w1", w_relay, 1, k)
-    plan("td", tok_diagonal, 0)
-    plan("w2", w_relay, 2, 2)
-    plan("w2", w_relay, 2, 3)
-    plan("td", tok_diagonal, 1)
-    plan("w2", w_relay, 2, 1)
-    for u in range(3, units):
-        for k in (2, 3, 1):
-            plan("w%d" % u, w_relay, u, k)
-    for k in (2, 3, 1):
-        plan("o", o_relay, k, 0)
-
-    upto("tx")
-    o_relay(0, 0)
-    o_relay(0, 1)
+    tok_z(0)
+    for part in range(pieces):
+        o_relay(0, part)
+    tok_z(1)
+    w_late()
+    for q in range(2):
+        tok_x(q)
+    w_relay_mid()
     scale(odd, c)
     for q in range(2):
         tok_arrive(3, q, odd, 1 - c, x)
         tok_arrive(5, q, odd, 1 - c, 1 - x)
     scale(odd, 1 - c)
-    upto("td")
+
+    def w_relays(u):
+        w_relay(u, 1)
+        w_relay_end(u)
+        w_relay(u, 3)
+
+    w_relays(0)
+    tok_diagonal(0)
+    w_relays(1)
+    tok_diagonal(1)
     scale(1 - odd, c)
     for q in range(2):
         tok_arrive(4, q, 1 - odd, 1 - c, x)
         tok_arrive(6, q, 1 - odd, 1 - c, 1 - x)
     scale(1 - odd, 1 - c)
+    w_relays(2)
 
     def project_units(first, count):
         def one(i, _):
@@ -974,15 +1014,12 @@
 
         lax.fori_loop(0, blocks, one, 0)
 
-    upto("w1")
     w_need(0)
     w_need(1)
     project_units(0, 2)
     for e, (zq, cc) in enumerate([(odd, 1 - c), (1 - odd, c), (1 - odd, 1 - c)]):
         arrive(extra.at[zq * 2 + cc], extra_send.at[e], extra_recv.at[e], other_c)
-    upto("w2")
-    w_need(2)
-    project_units(2, 1)
+    w_relays(3)
 
     rate = rate_ref[:, lanes(head)]
     series = jnp.ones_like(rate)
@@ -998,23 +1035,20 @@
     sub = lax.broadcasted_iota(jnp.int32, (eighths, 8, DK), 1)
     over_last = (((1,), (1,)), ((), ()))
     decays = []
-    for b in range(blocks):
+
+    def score_block(b):
         at = slice(b * block, (b + 1) * block)
         q = proj[1, at, :].astype(f32) * DK ** (-0.5)
         kg = keep * jax.nn.sigmoid(-proj[0, at, :].astype(f32))
-        v = proj[2, at, :]
         added = jnp.broadcast_to(extra[b, pl.ds(head, 1), :], (DK, block)).T
         logs = jnp.log1p(-kg) + added
         cum = jnp.dot(lower, logs, precision=coarsest_scale_depth, preferred_element_type=f32)
         last = cum[block - 1 :, :]
-        state[b] = lax.dot_general(
-            v,
-            (kg * jnp.exp(last - cum)).astype(bf16),
-            (((0,), (0,)), ((), ())),
-            preferred_element_type=f32,
-        )
+        faded[at, :] = (kg * jnp.exp(last - cum)).astype(bf16)
         decays.append(jnp.exp(last))
         reach[at, :] = (q * jnp.exp(cum)).astype(bf16)
+        kept[0, at, :] = cum
+        kept[1, at, :] = kg
         scores = jnp.zeros((block, block), f32)
         span = 8
         while span < block:
@@ -1028,10 +1062,19 @@
             found = lax.dot_general(probe, keyed, over_last, preferred_element_type=f32)
             scores = scores + jnp.where(row // twice == col // twice, found, 0.0)
             span = twice
-        result = jnp.dot(scores.astype(bf16), v, preferred_element_type=f32)
-        c3 = cum.reshape(eighths, 8, DK)
+        scored[b] = scores.astype(bf16)
+
+    def value_block(b):
+        at = slice(b * block, (b + 1) * block)
+        q = proj[1, at, :].astype(f32) * DK ** (-0.5)
+        v = proj[2, at, :]
+        state[b] = lax.dot_general(
+            v, faded[at, :], (((0,), (0,)), ((), ())), preferred_element_type=f32
+        )
+        result = jnp.dot(scored[b], v, preferred_element_type=f32)
+        c3 = kept[0, at, :].reshape(eighths, 8, DK)
         q3 = q.reshape(eighths, 8, DK)
-        k3 = kg.reshape(eighths, 8, DK)
+        k3 = kept[1, at, :].reshape(eighths, 8, DK)
         v3 = v.astype(f32).reshape(eighths, 8, DK)
         near = result.reshape(eighths, 8, DK)
         for s in range(8):
@@ -1039,12 +1082,18 @@
             score = jnp.sum(q3 * k3[:, s : s + 1, :] * weight, axis=2, keepdims=True)
             near = near + jnp.where(sub >= s, score * v3[:, s : s + 1, :], 0.0)
         local[at, :] = near.reshape(block, DK)
-        if b == 0:
-            upto("w3")
-        elif b == 1:
-            pump(1)
-        else:
-            pump(1)
+
+    score_block(0)
+    score_block(1)
+    w_need(2)
+    project_units(2, 1)
+    w_relays(4)
+    o_out(1)
+    o_out(2, is_mid)
+    score_block(2)
+    score_block(3)
+    for b in range(blocks):
+        value_block(b)
 
     sums = [decays[2 * i + 1] * state[2 * i] + state[2 * i + 1] for i in range(2)]
     fades = [decays[2 * i] * decays[2 * i + 1] for i in range(2)]
@@ -1058,7 +1107,7 @@
     for i in range(2):
         tail_go[i] = proj[3, (i + 1) * half - 16 : (i + 1) * half, :]
     send(tail_go, tail_come, scan_send.at[2], scan_recv.at[2], other_y)
-    upto("w4")
+    w_relays(5)
 
     arrive(state_come, scan_send.at[0], scan_recv.at[0], other_y)
     arrive(decay_come, scan_send.at[1], scan_recv.at[1], other_y)
@@ -1079,11 +1128,14 @@
     total_go[...] = total.astype(bf16)
     arrive(tail_come, scan_send.at[2], scan_recv.at[2], other_y)
     last_go[...] = jnp.where(first_y, tail_come[1].astype(f32), tail_go[1].astype(f32)).astype(bf16)
-    across = peer(slabs[2], y, c)
+    across = peer((z + 2) % 4, y, c)
     send(total_go, total_come, scan_send.at[3], scan_recv.at[3], across)
     send(last_go, last_come, scan_send.at[4], scan_recv.at[4], across)
 
-    upto("w5")
+    o_out(2, is_end, range(2))
+    o_out(3, is_mid)
+    for part in range(pieces):
+        o_relay(1, part)
     w_need(4)
     w_need(5)
     project_units(4, 2)
@@ -1157,8 +1209,10 @@
         )
         at = y_all.at[part * 4 + head]
         send(at, at, y_send.at[1, part], y_recv.at[1, part], other_c)
-    o_out(1)
-    upto("o")
+    o_out(2, is_end, range(2, pieces))
+    o_out(3, is_end)
+    for part in range(pieces):
+        o_relay(2, part)
     for part in range(2):
         at = y_all.at[part * 4 + their_head]
         arrive(at, y_send.at[0, part], y_recv.at[0, part], z_peer)
@@ -1177,8 +1231,6 @@
         return own_rows(cc * rows + xx * owned, owned)
 
     def out_chunk(k):
-        if k > 0:
-            o_relay(k, 1)
         o_need(k)
         left = jnp.concatenate([y_all[i] for i in range(8)], axis=1)
         right = jnp.concatenate([o_all[slabs[k] * 2], o_all[slabs[k] * 2 + 1]], axis=1)
@@ -1202,18 +1254,27 @@
             mine[:, lanes(slabs[k] * 4 + yy * 2 + c)] = ours[:, cols]
             mine[:, lanes(slabs[k] * 4 + yy * 2 + 1 - c)] = others[:, cols]
 
-    turns = (0, 2, 3, 1)
-    for turn, k in enumerate(turns):
-        out_chunk(k)
-        if turn > 0:
-            gather_chunk(turns[turn - 1])
-    gather_chunk(turns[-1])
+    out_chunk(0)
+    out_chunk(1)
+    for part in range(2):
+        o_relay(3, part)
+    out_chunk(2)
+    for part in range(2, pieces):
+        o_relay(3, part)
+    for k in range(3):
+        gather_chunk(k)
+    out_chunk(3)
+    gather_chunk(3)
     summed = mine[...]
     out_ref[...] = (
         summed
         * lax.rsqrt(jnp.mean(summed * summed, axis=1, keepdims=True) + eps)
         * post_ref[...]
     ).astype(bf16)
+    for u in range(units):
+        for k in range(4):
+            at = w_all.at[u, w_piece(slabs[k], 0, 2)]
+            send_copy(at, at, wy_send.at[u, k], wy_recv.at[u, k], other_y).wait_send()
     for copy in sends:
         copy.wait_send()
 
@@ -1262,6 +1323,9 @@
             pltpu.VMEM((units, positions, DK), bf16),
             pltpu.VMEM((positions, DK), f32),
             pltpu.VMEM((positions, DK), bf16),
+            pltpu.VMEM((positions, DK), bf16),
+            pltpu.VMEM((2, positions, DK), f32),
+            pltpu.VMEM((4, rows, rows), bf16),
             pltpu.VMEM((4, DK, DK), f32),
             pltpu.VMEM((2, DK, DK), bf16),
             pltpu.VMEM((2, DK, DK), bf16),
@@ -1287,10 +1351,10 @@
             dma((units, slabs, 2)),
             dma((units, slabs)),
             dma((units, slabs)),
-            dma((slabs, 2)),
-            dma((slabs, 2)),
-            dma((slabs, 2)),
-            dma((slabs, 2)),
+            dma((slabs, 4)),
+            dma((slabs, 4)),
+            dma((slabs, 4)),
+            dma((slabs, 4)),
             dma((5,)),
             dma((5,)),
             dma((3, 2)),

time: 111 us -> 91.4 us (0.82)
  the two profiles are of different devices: /device:TPU:9 before, /device:TPU:0 now
where the time goes in v2:
time: 91.4 us; the launch traced here: 91.2 us
  Pallas kernels  89.3 us (98%)
  local copies, waits for them, and re-layouts  1.88 us (2%)
    pallas_call x1, Pallas kernels, pair_layer(): pl.pallas_call(pair_kernel, out_shape=jax.ShapeDtypeStruct((owned, model)...  89.3 us
    unnamed x1, local copies, waits for them, and re-layouts  1.88 us

profile of v2, /device:TPU:0, one launch (start us, length us, event | category | flops | bytes accessed | tf_op | source)
XLA Modules:
  0.0 91.2 jit_solution(9291770401397198135)
XLA Ops:
  0.0 89.3 %shard_map.154 = bf16[128,2048]{1,0:T(8,128)(2,1)} custom-call(bf16[256,1024]{1,0:T(8,128)(2,1)} %tok_hbm.1, f32[1,2048]{1,0:T(1,128)} %bitcast.6, bf16[128,512]{1,0:T(8,128)(2,1)} %w0.1, bf16[128,512]{1,0:T(8,128)(2,1)} %w1.1, bf16[128,512]{1,0:T(8,128)(2,1)} %w2.1, bf16[128,512]{1,0:T(8,128)(2,1)} %w3.1, bf16[128,512]{1,0:T(8,128)(2,1)} %w4.1, ...), custom_call_target="tpu_custom_call" | custom-call | flops 3221225472 | bytes 1572864 | tf_op jit(solution)/shard_map/pallas_call | solution.py:1309
  89.3 1.9 %copy.18 = bf16[128,2048]{1,0:T(8,128)(2,1)} copy(bf16[128,2048]{1,0:T(8,128)(2,1)} %shard_map.154) | data formatting | bytes 1048576

commit v3 on v2

--- a/solution.py
+++ b/solution.py
@@ -698,13 +698,13 @@
     tail_come,
     total_go,
     total_come,
-    last_go,
     last_come,
     y_all,
     y_go,
     part_go,
     part_come,
     mine,
+    done,
     own_sem,
     tok_send,
     tok_recv,
@@ -733,6 +733,7 @@
     pair = z // 2
     head = odd * 2 + c
     is_mid = (z == 1) | (z == 2)
+    is_end = jnp.logical_not(is_mid)
     slabs = [z, z + 1 - 2 * odd, 2 - pair, 3 * (1 - pair)]
     my_slot = jnp.where(is_mid, 2, 3)
     rows, feats = tok_hbm.shape
@@ -743,7 +744,9 @@
     half = positions // 2
     block = rows
     blocks = positions // block
-    piece = rows // 2
+    n_rows = w_all.shape[1]
+    tok_pieces = 4
+    piece = rows // tok_pieces
 
     def peer(zz, yy, cc):
         return {"sp": zz * 4 + yy * 2 + cc}
@@ -771,51 +774,63 @@
         copy.start()
         owns[name] = copy
 
-    for q in range(2):
-        own_copy(("tok", q), tok_hbm.at[pl.ds(q * piece, piece)], tok_at(odd, c, x, q))
-    for u, part in enumerate(parts):
-        own_copy(("w", u), part, w_own.at[u])
+    own_tok = wide.at[
+        own_rows(odd * half + c * rows, rows), pl.ds(pl.multiple_of(x * feats, 128), feats)
+    ]
+    own_copy("tok", tok_hbm, own_tok)
     own_copy("extra", extra_hbm, extra.at[odd * 2 + c])
     here = z * 2 + y
-    own_copy(("o", 0), orec_hbm, o_all.at[here, pl.ds(0, 4 * DK)])
-    own_copy(("o", 1), opool_hbm, o_all.at[here, pl.ds(4 * DK, 4 * DK)])
-    own_copy("mix", mix_hbm.at[head], mix_own)
+    w_landed = own_sem.at[2]
+    for u, part in enumerate(parts):
+        pltpu.make_async_copy(part, w_own.at[u], w_landed).start()
+    o_landed = own_sem.at[3]
+    pltpu.make_async_copy(orec_hbm, o_all.at[here, pl.ds(0, 4 * DK)], o_landed).start()
+    pltpu.make_async_copy(opool_hbm, o_all.at[here, pl.ds(4 * DK, 4 * DK)], o_landed).start()
+    mix_copy = pltpu.make_async_copy(mix_hbm.at[head], mix_own, own_sem.at[4])
+    mix_copy.start()
 
     barrier = pltpu.get_barrier_semaphore()
-    peers = [other_c, other_y, peer_x(c), peer_x(1 - c)]
+    across = peer((z + 2) % 4, y, c)
+    across_y = peer((z + 2) % 4, 1 - y, c)
+    peers = [other_c, other_y, peer_x(c), peer_x(1 - c), across_y]
     for k in range(1, 4):
         peers += [peer(slabs[k], y, c), peer(slabs[k], y, 1 - c)]
     for to in peers:
         pl.semaphore_signal(barrier, inc=1, device_id=to)
     pl.semaphore_wait(barrier, len(peers))
 
-    sends = []
-
     def send(src, dst, send_sem, recv_sem, to):
-        copy = pltpu.make_async_remote_copy(
+        pltpu.make_async_remote_copy(
             src_ref=src, dst_ref=dst, send_sem=send_sem, recv_sem=recv_sem, device_id=to
-        )
-        copy.start()
-        sends.append(copy)
-
-    def arrive(dst, send_sem, recv_sem, to):
+        ).start()
+
+    def sent(ref, send_sem):
         pltpu.make_async_remote_copy(
-            src_ref=dst, dst_ref=dst, send_sem=send_sem, recv_sem=recv_sem, device_id=to
+            src_ref=ref, dst_ref=ref, send_sem=send_sem, recv_sem=send_sem, device_id=other_c
+        ).wait_send()
+
+    def arrive(ref, recv_sem):
+        pltpu.make_async_remote_copy(
+            src_ref=ref, dst_ref=ref, send_sem=recv_sem, recv_sem=recv_sem, device_id=other_c
         ).wait_recv()
 
-    def tok_send_to(kind, q, zq, cc, xx, to):
-        at = tok_at(zq, cc, xx, q)
-        send(at, at, tok_send.at[kind, q], tok_recv.at[kind, q], to)
-
-    def tok_arrive(kind, q, zq, cc, xx):
-        at = tok_at(zq, cc, xx, q)
-        arrive(at, tok_send.at[kind, q], tok_recv.at[kind, q], other_c)
-
-    for q in range(2):
-        owns[("tok", q)].wait()
-        tok_send_to(0, q, odd, c, x, peer(slabs[1], y, c))
-        tok_send_to(1, q, odd, c, x, peer_x(c))
-        tok_send_to(3, q, odd, c, x, other_c)
+    def tok_rows(zq, cc, xx):
+        start = zq * half + cc * rows
+        return wide.at[own_rows(start, rows), pl.ds(pl.multiple_of(xx * feats, 128), feats)]
+
+    def tok_share(at, near):
+        send(at, at, tok_send.at[1], tok_recv.at[9 if near else 10], other_c)
+
+    owns["extra"].wait()
+    for e, to in enumerate([other_c, peer(slabs[1], y, c), peer(slabs[1], y, 1 - c)]):
+        at = extra.at[odd * 2 + c]
+        send(at, at, extra_send.at[0], extra_recv.at[e], to)
+    owns["tok"].wait()
+    for q in range(tok_pieces):
+        at = tok_at(odd, c, x, q)
+        send(at, at, tok_send.at[0], tok_recv.at[q], peer(slabs[1], y, c))
+    send(own_tok, own_tok, tok_send.at[1], tok_recv.at[8], peer_x(c))
+    tok_share(own_tok, True)
 
     def w_piece(slab, cc, n=1):
         return own_rows((slab * 4 + y * 2 + cc) * shard, n * shard)
@@ -834,14 +849,14 @@
                 send_copy(
                     w_own.at[u, :, lanes((slabs[k] % 2) * 2 + cc)],
                     w_all.at[u, w_piece(z, c)],
-                    w_send.at[u, k, e],
-                    w_recv.at[u, slot, e],
+                    w_send.at[0],
+                    w_recv.at[u, slot],
                     peer(slabs[k], y, cc),
                 )
             )
-        issue(copies, only, last=only is not is_mid)
-
-    def issue(copies, only=None, last=True):
+        issue(copies, only)
+
+    def issue(copies, only=None):
         if only is None:
             for copy in copies:
                 copy.start()
@@ -852,115 +867,120 @@
                 for copy in copies:
                     copy.start()
 
-        if last:
-            sends.extend(copies)
-
-    w_locals = []
+    pltpu.make_async_copy(w_own, w_own, w_landed).wait()
     for u in range(units):
-        owns[("w", u)].wait()
-        keep_here = pltpu.make_async_copy(
-            w_own.at[u, :, lanes(head)], w_all.at[u, w_piece(z, c)], own_sem.at[len(owns) + u]
-        )
-        keep_here.start()
-        w_locals.append(keep_here)
+        pltpu.make_async_copy(
+            w_own.at[u, :, lanes(head)], w_all.at[u, w_piece(z, c)], w_recv.at[u, 0]
+        ).start()
         send(
             w_own.at[u, :, lanes(odd * 2 + 1 - c)],
             w_all.at[u, w_piece(z, c)],
-            w_send.at[u, 0, 1],
-            w_recv.at[u, 0, 1],
+            w_send.at[0],
+            w_recv.at[u, 0],
             other_c,
         )
-        w_send_to(u, 1)
-    for u in range(units):
+        w_send_to(u, 1, None if u == 0 else is_mid)
         w_send_to(u, 2, is_mid)
-    owns["extra"].wait()
-    for e, to in enumerate([other_c, peer(slabs[1], y, c), peer(slabs[1], y, 1 - c)]):
-        at = extra.at[odd * 2 + c]
-        send(at, at, extra_send.at[e], extra_recv.at[e], to)
 
     def w_relay(u, k):
-        if k == 0:
-            w_locals[u].wait()
-        else:
-            arrive(
-                w_all.at[u, w_piece(slabs[k], c)], w_send.at[u, k, 0], w_recv.at[u, k, 0], other_c
-            )
-        arrive(
-            w_all.at[u, w_piece(slabs[k], 1 - c)], w_send.at[u, k, 1], w_recv.at[u, k, 1], other_c
-        )
         at = w_all.at[u, w_piece(slabs[k], 0, 2)]
-        send_copy(at, at, wy_send.at[u, k], wy_recv.at[u, k], other_y).start()
-
-    def w_relay_mid():
+        arrive(at, w_recv.at[u, k])
+        send(at, at, wy_send.at[0], wy_recv.at[u], other_y)
+
+    def w_late_end():
+        for u in range(units):
+            w_send_to(u, 3, is_end)
+            w_send_to(u, 2, is_end)
+            if u > 0:
+                w_send_to(u, 1, is_end)
+
+    def w_late_mid():
+        for u in range(units):
+            w_send_to(u, 3, is_mid)
+
+    def w_need(u):
+        arrive(w_all.at[u, pl.ds(0, n_rows // 2)], wy_recv.at[u])
+
+    pieces = 4
+    depth = o_all.shape[1] // pieces
+
+    def o_at(slab, yy, part):
+        return o_all.at[slab * 2 + yy, pl.ds(part * depth, depth)]
+
+    def o_copy(route, part, held, slot, to):
+        at = o_at(held, y, part)
+        return send_copy(
+            at, at, o_send.at[min(route, 1)], o_recv.at[slot - 1, part], peer(to, y, c)
+        )
+
+    def o_near():
+        for part in range(pieces):
+            o_copy(0, part, z, 1, slabs[1]).start()
+
+    def o_across(which):
         @pl.when(is_mid)
         def _():
-            for u in range(units):
-                w_relay(u, 2)
-
-    def w_relay_end(u):
-        @pl.when(jnp.logical_not(is_mid))
-        def _():
-            w_relay(u, 2)
-
-    def w_late():
-        for u in range(units):
-            w_send_to(u, 2, jnp.logical_not(is_mid))
-            w_send_to(u, 3)
-
-    def w_need(u):
-        for k in range(4):
-            start = (slabs[k] * 4 + (1 - y) * 2) * shard
-            at = w_all.at[u, own_rows(start, 2 * shard)]
-            arrive(at, wy_send.at[u, k], wy_recv.at[u, k], other_y)
-
-    pieces = 4
-    depth = o_all.shape[1] // pieces
-
-    def o_at(slab, yy, part):
-        return o_all.at[slab * 2 + yy, pl.ds(part * depth, depth)]
-
-    def o_out(k, only=None, which=range(pieces)):
-        slot = 1 if k == 1 else my_slot
-        copies = []
-        for part in which:
-            at = o_at(z, y, part)
-            copies.append(
-                send_copy(
-                    at, at, o_send.at[k, part], o_recv.at[slot, part], peer(slabs[k], y, c)
-                )
-            )
-        issue(copies, only, last=only is not is_mid)
+            for part in which:
+                o_copy(1, part, z, 2, slabs[2]).start()
 
     def o_relay(k, part):
         at = o_at(slabs[k], y, part)
         if k > 0:
-            arrive(at, o_send.at[k, part], o_recv.at[k, part], other_c)
-        send(at, at, oy_send.at[k, part], oy_recv.at[k, part], other_y)
+            arrive(at, o_recv.at[k - 1, part])
+        send(at, at, oy_send.at[0], oy_recv.at[k], other_y)
+
+    def o_onward(k, part):
+        if k == 1:
+            o_copy(2, part, slabs[1], 3, slabs[2]).start()
+        else:
+            o_copy(k + 1, part, slabs[k], k, slabs[1]).start()
+
+    def o_near_relays(which):
+        for part in which:
+            o_relay(1, part)
+
+            @pl.when(is_mid)
+            def _():
+                o_onward(1, part)
+
+    def o_mid_relays(k, which):
+        @pl.when(is_mid)
+        def _():
+            for part in which:
+                o_relay(k, part)
+                o_onward(k, part)
+
+    def o_end_relays(k, which):
+        @pl.when(is_end)
+        def _():
+            for part in which:
+                o_relay(k, part)
 
     def o_need(k):
-        for part in range(pieces):
-            at = o_at(slabs[k], 1 - y, part)
-            arrive(at, oy_send.at[k, part], oy_recv.at[k, part], other_y)
-
-    is_end = jnp.logical_not(is_mid)
+        arrive(o_all.at[slabs[k] * 2 + 1 - y], oy_recv.at[k])
 
     for u in range(units):
         w_relay(u, 0)
-    for part in range(2):
-        owns[("o", part)].wait()
+    pltpu.make_async_copy(o_all.at[here], o_all.at[here], o_landed).wait()
 
     def tok_z(q):
-        tok_arrive(0, q, 1 - odd, c, x)
-        tok_send_to(2, q, 1 - odd, c, x, peer_x(c))
-        tok_send_to(4, q, 1 - odd, c, x, other_c)
-
-    def tok_x(q):
-        tok_arrive(1, q, odd, c, 1 - x)
-        tok_send_to(5, q, odd, c, 1 - x, other_c)
+        at = tok_at(1 - odd, c, x, q)
+        arrive(at, tok_recv.at[q])
+        send(at, at, tok_send.at[1], tok_recv.at[4 + q], peer_x(c))
+        tok_share(at, False)
+
+    def tok_x():
+        at = tok_rows(odd, c, 1 - x)
+        arrive(at, tok_recv.at[8])
+        tok_share(at, True)
 
     def tok_diagonal(q):
-        tok_arrive(2, q, 1 - odd, c, 1 - x)
-        tok_send_to(6, q, 1 - odd, c, 1 - x, other_c)
+        at = tok_at(1 - odd, c, 1 - x, q)
+        arrive(at, tok_recv.at[4 + q])
+        tok_share(at, False)
+
+    def tok_shared(zq, near):
+        arrive(wide.at[own_rows(zq * half + (1 - c) * rows, rows)], tok_recv.at[9 if near else 10])
 
     def scale(zq, cc):
         at = own_rows(zq * half + cc * rows, rows)
@@ -971,33 +991,34 @@
             lax.rsqrt(squares / wide.shape[1] + eps), (rows, DK)
         )
 
+    def w_relays(u):
+        w_relay(u, 1)
+        w_relay(u, 2)
+        w_relay(u, 3)
+
     tok_z(0)
+    tok_z(1)
+    w_late_end()
     for part in range(pieces):
         o_relay(0, part)
-    tok_z(1)
-    w_late()
-    for q in range(2):
-        tok_x(q)
-    w_relay_mid()
+    tok_z(2)
+    sent(own_tok, tok_send.at[0])
+    w_late_mid()
+    tok_z(3)
+    tok_x()
     scale(odd, c)
-    for q in range(2):
-        tok_arrive(3, q, odd, 1 - c, x)
-        tok_arrive(5, q, odd, 1 - c, 1 - x)
+    tok_shared(odd, True)
     scale(odd, 1 - c)
-
-    def w_relays(u):
-        w_relay(u, 1)
-        w_relay_end(u)
-        w_relay(u, 3)
-
-    w_relays(0)
+    w_relay(0, 2)
+    w_relay(0, 1)
+    w_relay(0, 3)
     tok_diagonal(0)
+    tok_diagonal(1)
     w_relays(1)
-    tok_diagonal(1)
+    tok_diagonal(2)
+    tok_diagonal(3)
     scale(1 - odd, c)
-    for q in range(2):
-        tok_arrive(4, q, 1 - odd, 1 - c, x)
-        tok_arrive(6, q, 1 - odd, 1 - c, 1 - x)
+    tok_shared(1 - odd, False)
     scale(1 - odd, 1 - c)
     w_relays(2)
 
@@ -1018,8 +1039,7 @@
     w_need(1)
     project_units(0, 2)
     for e, (zq, cc) in enumerate([(odd, 1 - c), (1 - odd, c), (1 - odd, 1 - c)]):
-        arrive(extra.at[zq * 2 + cc], extra_send.at[e], extra_recv.at[e], other_c)
-    w_relays(3)
+        arrive(extra.at[zq * 2 + cc], extra_recv.at[e])
 
     rate = rate_ref[:, lanes(head)]
     series = jnp.ones_like(rate)
@@ -1084,16 +1104,19 @@
         local[at, :] = near.reshape(block, DK)
 
     score_block(0)
+    w_relays(3)
     score_block(1)
+    score_block(2)
+    score_block(3)
+    w_relays(4)
+    o_near()
+    o_across(range(2))
     w_need(2)
     project_units(2, 1)
-    w_relays(4)
-    o_out(1)
-    o_out(2, is_mid)
-    score_block(2)
-    score_block(3)
     for b in range(blocks):
         value_block(b)
+        if b == 2:
+            w_relays(5)
 
     sums = [decays[2 * i + 1] * state[2 * i] + state[2 * i + 1] for i in range(2)]
     fades = [decays[2 * i] * decays[2 * i + 1] for i in range(2)]
@@ -1107,10 +1130,12 @@
     for i in range(2):
         tail_go[i] = proj[3, (i + 1) * half - 16 : (i + 1) * half, :]
     send(tail_go, tail_come, scan_send.at[2], scan_recv.at[2], other_y)
-    w_relays(5)
-
-    arrive(state_come, scan_send.at[0], scan_recv.at[0], other_y)
-    arrive(decay_come, scan_send.at[1], scan_recv.at[1], other_y)
+    send(tail_go.at[1], last_come, scan_send.at[4], scan_recv.at[4], across_y)
+    w_need(4)
+    project_units(4, 1)
+
+    arrive(state_come, scan_recv.at[0])
+    arrive(decay_come, scan_recv.at[1])
     first_y = y == 0
     theirs = [state_come[i].astype(f32) for i in range(2)]
     their_fades = [decay_come[i : i + 1, :] for i in range(2)]
@@ -1126,22 +1151,13 @@
     for add, fade in order[1:]:
         total = fade * total + add
     total_go[...] = total.astype(bf16)
-    arrive(tail_come, scan_send.at[2], scan_recv.at[2], other_y)
-    last_go[...] = jnp.where(first_y, tail_come[1].astype(f32), tail_go[1].astype(f32)).astype(bf16)
-    across = peer((z + 2) % 4, y, c)
     send(total_go, total_come, scan_send.at[3], scan_recv.at[3], across)
-    send(last_go, last_come, scan_send.at[4], scan_recv.at[4], across)
-
-    o_out(2, is_end, range(2))
-    o_out(3, is_mid)
-    for part in range(pieces):
-        o_relay(1, part)
-    w_need(4)
-    w_need(5)
-    project_units(4, 2)
-    owns["mix"].wait()
-    arrive(total_come, scan_send.at[3], scan_recv.at[3], across)
-    arrive(last_come, scan_send.at[4], scan_recv.at[4], across)
+    o_across(range(2, pieces))
+    o_near_relays(range(2))
+    o_mid_relays(2, range(2))
+    mix_copy.wait()
+    arrive(tail_come, scan_recv.at[2])
+    arrive(last_come, scan_recv.at[4])
 
     later_pair = pair > 0
     at_head = lanes(head)
@@ -1152,15 +1168,9 @@
     line_half = lax.broadcasted_iota(jnp.int32, (half, DK), 0)
     far = [jnp.where(later_pair, last_come[...].astype(f32), 0.0), tail_come[0].astype(f32)]
     their_tails = [tail_come[i].astype(f32) for i in range(2)]
-    befores = []
-    running = jnp.where(later_pair, total_come[...].astype(f32), 0.0)
-    for i in range(2):
-        after_first = order[2 * i][1] * running + order[2 * i][0]
-        befores.append(jnp.where(first_y, running, after_first))
-        running = order[2 * i + 1][1] * after_first + order[2 * i + 1][0]
-
-    def y_half(i):
-        at = own_rows(i * half, half)
+    is_odd = odd == 1
+
+    def pool_half(i):
         at_static = slice(i * half, (i + 1) * half)
         xin = proj[3, at_static, :].astype(f32)
         prior = jnp.where(first_y, far[i], their_tails[i])
@@ -1173,110 +1183,173 @@
         count = jnp.minimum(begins + line_half + 1, window).astype(f32)
         mixed = (chosen / count - xin).astype(bf16)
         mapped = jnp.dot(mixed, mix_own[...], preferred_element_type=f32)
-        gate = proj[5, at_static, :].astype(f32)
-        pooled = (mapped * pgain_ref[:, at_head] * (gate * jax.nn.sigmoid(gate))).astype(bf16)
-        cur = befores[i]
-        recs = []
-        for j in range(2):
-            b = 2 * i + j
-            rows_b = slice(b * block, (b + 1) * block)
-            rec = local[rows_b, :] + lax.dot_general(
-                reach[rows_b, :], cur.astype(bf16), over_last, preferred_element_type=f32
-            )
-            cur = decays[b] * cur + state[b]
-            normed = rec * lax.rsqrt(jnp.mean(rec * rec, axis=1, keepdims=True) + eps)
-            gate = proj[4, rows_b, :].astype(f32)
-            recs.append(
-                (normed * sgain_ref[:, at_head] * (gate * jax.nn.sigmoid(gate))).astype(bf16)
-            )
-        return jnp.concatenate(recs, axis=0), pooled
-
-    halves = [y_half(i) for i in range(2)]
-    is_odd = odd == 1
-    for part in range(2):
-        low, high = halves[0][part].astype(f32), halves[1][part].astype(f32)
-        y_go[part] = jnp.where(is_odd, low, high).astype(bf16)
-        y_all[part * 4 + head] = jnp.where(is_odd, high, low).astype(bf16)
+        gate = proj[4, at_static, :].astype(f32)
+        return mapped * pgain_ref[:, at_head] * (gate * jax.nn.sigmoid(gate))
+
     z_peer = peer(slabs[1], y, c)
     their_head = (1 - odd) * 2 + c
-    for part in range(2):
+
+    def y_at(part, hd, ch):
+        return y_all.at[part * 4 + hd, pl.ds(ch * block, block)]
+
+    def y_put(part, ch, low, high):
+        at = slice(ch * block, (ch + 1) * block)
+        y_go[part, at, :] = jnp.where(is_odd, low, high).astype(bf16)
+        y_all[part * 4 + head, at, :] = jnp.where(is_odd, high, low).astype(bf16)
         send(
-            y_go.at[part],
-            y_all.at[part * 4 + head],
-            y_send.at[0, part],
-            y_recv.at[0, part],
+            y_go.at[part, pl.ds(ch * block, block)],
+            y_at(part, head, ch),
+            y_send.at[0],
+            y_recv.at[part * 2 + ch],
             z_peer,
         )
-        at = y_all.at[part * 4 + head]
-        send(at, at, y_send.at[1, part], y_recv.at[1, part], other_c)
-    o_out(2, is_end, range(2, pieces))
-    o_out(3, is_end)
-    for part in range(pieces):
-        o_relay(2, part)
-    for part in range(2):
-        at = y_all.at[part * 4 + their_head]
-        arrive(at, y_send.at[0, part], y_recv.at[0, part], z_peer)
-        send(at, at, y_send.at[2, part], y_recv.at[2, part], other_c)
-    for part in range(2):
-        at = y_all.at[part * 4 + odd * 2 + 1 - c]
-        arrive(at, y_send.at[1, part], y_recv.at[1, part], other_c)
-    for part in range(2):
-        at = y_all.at[part * 4 + (1 - odd) * 2 + 1 - c]
-        arrive(at, y_send.at[2, part], y_recv.at[2, part], other_c)
+        at = y_at(part, head, ch)
+        send(at, at, y_send.at[0], y_recv.at[4 + ch], other_c)
+
+    def y_pass(part, ch):
+        at = y_at(part, their_head, ch)
+        arrive(at, y_recv.at[part * 2 + ch])
+        send(at, at, y_send.at[0], y_recv.at[4 + ch], other_c)
+
+    def y_need(ch):
+        arrive(y_all.at[pl.ds(0, 2)], y_recv.at[4 + ch])
+
+    pooled = [pool_half(i) for i in range(2)]
+    for ch in range(2):
+        rows_ch = slice(ch * block, (ch + 1) * block)
+        y_put(1, ch, pooled[0][rows_ch], pooled[1][rows_ch])
+    o_near_relays(range(2, pieces))
+    w_need(5)
+    project_units(5, 1)
+    arrive(total_come, scan_recv.at[3])
+    befores = []
+    running = jnp.where(later_pair, total_come[...].astype(f32), 0.0)
+    for i in range(2):
+        after_first = order[2 * i][1] * running + order[2 * i][0]
+        befores.append(jnp.where(first_y, running, after_first))
+        running = order[2 * i + 1][1] * after_first + order[2 * i + 1][0]
+
+    def rec_rows(b, before):
+        rows_b = slice(b * block, (b + 1) * block)
+        rec = local[rows_b, :] + lax.dot_general(
+            reach[rows_b, :], before.astype(bf16), over_last, preferred_element_type=f32
+        )
+        normed = rec * lax.rsqrt(jnp.mean(rec * rec, axis=1, keepdims=True) + eps)
+        gate = proj[5, rows_b, :].astype(f32)
+        return normed * sgain_ref[:, at_head] * (gate * jax.nn.sigmoid(gate))
+
+    for ch in range(2):
+        recs = []
+        for i in range(2):
+            b = 2 * i + ch
+            recs.append(rec_rows(b, befores[i]))
+            befores[i] = decays[b] * befores[i] + state[b]
+        y_put(0, ch, recs[0], recs[1])
+    o_mid_relays(2, range(2, pieces))
+    for ch in range(2):
+        y_pass(1, ch)
+    o_mid_relays(3, range(2))
+    o_end_relays(2, range(2))
+    y_pass(0, 0)
+    o_mid_relays(3, range(2, pieces))
+    o_end_relays(2, range(2, pieces))
+    y_pass(0, 1)
 
     owned = part_come.shape[2]
-    part_peers = [(x, 1 - c, other_c), (1 - x, c, peer_x(c)), (1 - x, 1 - c, peer_x(1 - c))]
 
     def rows_for(xx, cc):
         return own_rows(cc * rows + xx * owned, owned)
 
-    def out_chunk(k):
-        o_need(k)
-        left = jnp.concatenate([y_all[i] for i in range(8)], axis=1)
+    def part_copies(k, ch):
+        over_x = send_copy(
+            part_go.at[k, rows_for(1 - x, ch)],
+            part_come.at[k, c],
+            part_send.at[0],
+            part_recv.at[k],
+            peer_x(ch),
+        )
+        over_c = send_copy(
+            part_go.at[k, rows_for(x, ch)],
+            part_come.at[k, 2],
+            part_send.at[0],
+            part_recv.at[k],
+            other_c,
+        )
+        return over_x, over_c
+
+    def out_chunk(k, ch):
+        left = jnp.concatenate(
+            [y_all[i, ch * block : (ch + 1) * block, :] for i in range(8)], axis=1
+        )
         right = jnp.concatenate([o_all[slabs[k] * 2], o_all[slabs[k] * 2 + 1]], axis=1)
-        part_go[k] = jnp.dot(left, right, preferred_element_type=f32).astype(bf16)
-        for i, (xx, cc, to) in enumerate(part_peers):
-            send(
-                part_go.at[k, rows_for(xx, cc)],
-                part_come.at[k, i],
-                part_send.at[k, i],
-                part_recv.at[k, i],
-                to,
-            )
+        part_go[k, ch * block : (ch + 1) * block, :] = jnp.dot(
+            left, right, preferred_element_type=f32
+        ).astype(bf16)
+        over_x, over_c = part_copies(k, ch)
+        over_x.start()
+
+        @pl.when(c != ch)
+        def _():
+            over_c.start()
 
     def gather_chunk(k):
-        for i, (xx, cc, to) in enumerate(part_peers):
-            arrive(part_come.at[k, i], part_send.at[k, i], part_recv.at[k, i], to)
-        ours = part_go[k, rows_for(x, c), :].astype(f32) + part_come[k, 1].astype(f32)
-        others = part_come[k, 0].astype(f32) + part_come[k, 2].astype(f32)
+        arrive(part_come.at[k], part_recv.at[k])
+        ours = part_go[k, rows_for(x, c), :].astype(f32) + part_come[k, c].astype(f32)
+        others = part_come[k, 2].astype(f32) + part_come[k, 1 - c].astype(f32)
         for yy in range(2):
             cols = slice(yy * DK, (yy + 1) * DK)
             mine[:, lanes(slabs[k] * 4 + yy * 2 + c)] = ours[:, cols]
             mine[:, lanes(slabs[k] * 4 + yy * 2 + 1 - c)] = others[:, cols]
 
-    out_chunk(0)
-    out_chunk(1)
-    for part in range(2):
-        o_relay(3, part)
-    out_chunk(2)
-    for part in range(2, pieces):
-        o_relay(3, part)
-    for k in range(3):
+    for ch in range(2):
+        y_need(ch)
+        for k in range(2):
+            if ch == 0:
+                o_need(k)
+            out_chunk(k, ch)
+    o_need(2)
+    for ch in range(2):
+        o_end_relays(3, range(ch, ch + 1))
+        out_chunk(2, ch)
+    for k in range(2):
         gather_chunk(k)
-    out_chunk(3)
+        o_end_relays(3, range(k + 2, k + 3))
+    gather_chunk(2)
+    o_need(3)
+    for ch in range(2):
+        out_chunk(3, ch)
     gather_chunk(3)
-    summed = mine[...]
-    out_ref[...] = (
-        summed
-        * lax.rsqrt(jnp.mean(summed * summed, axis=1, keepdims=True) + eps)
-        * post_ref[...]
-    ).astype(bf16)
-    for u in range(units):
-        for k in range(4):
-            at = w_all.at[u, w_piece(slabs[k], 0, 2)]
-            send_copy(at, at, wy_send.at[u, k], wy_recv.at[u, k], other_y).wait_send()
-    for copy in sends:
-        copy.wait_send()
+
+    def finish():
+        summed = mine[...]
+        done[...] = (
+            summed
+            * lax.rsqrt(jnp.mean(summed * summed, axis=1, keepdims=True) + eps)
+            * post_ref[...]
+        ).astype(bf16)
+        copy = pltpu.make_async_copy(done, out_ref, own_sem.at[0])
+        copy.start()
+        copy.wait()
+
+    finish()
+    def drain():
+        sent(wide.at[pl.ds(0, 6 * rows // 2)], tok_send.at[1])
+        sent(extra.at[pl.ds(0, 3)], extra_send.at[0])
+        sent(w_all.at[pl.ds(0, 3), pl.ds(0, 14 * shard)], w_send.at[0])
+        sent(w_all.at[pl.ds(0, 3)], wy_send.at[0])
+        sent(o_all.at[0], o_send.at[0])
+        sent(o_all.at[pl.ds(0, 4)], oy_send.at[0])
+
+        @pl.when(is_mid)
+        def _():
+            sent(o_all.at[pl.ds(0, 4)], o_send.at[1])
+
+        for i, ref in enumerate([state_go, decay_go, tail_go, total_go, tail_go.at[1]]):
+            sent(ref, scan_send.at[i])
+        sent(y_all.at[pl.ds(0, 6)], y_send.at[0])
+        sent(part_go.at[pl.ds(0, 3)], part_send.at[0])
+
+    drain()
 
 
 def pair_layer(
@@ -1310,7 +1383,7 @@
         pair_kernel,
         out_shape=jax.ShapeDtypeStruct((owned, model), bf16),
         in_specs=[hbm, vmem] + [hbm] * 6 + [vmem, hbm, vmem, hbm, vmem, hbm, hbm, vmem],
-        out_specs=vmem,
+        out_specs=hbm,
         scratch_shapes=[
             pltpu.VMEM((positions, n_tp * feats), bf16),
             pltpu.VMEM((positions, n_tp * feats), bf16),
@@ -1336,31 +1409,31 @@
             pltpu.VMEM((DK, DK), bf16),
             pltpu.VMEM((DK, DK), bf16),
             pltpu.VMEM((16, DK), bf16),
-            pltpu.VMEM((16, DK), bf16),
             pltpu.VMEM((2 * heads, half, DK), bf16),
             pltpu.VMEM((2, half, DK), bf16),
             pltpu.VMEM((slabs, half, 2 * width), bf16),
             pltpu.VMEM((slabs, 3, owned, 2 * width), bf16),
             pltpu.VMEM((owned, model), f32),
-            dma((2 * units + 6,)),
-            dma((7, 2)),
-            dma((7, 2)),
+            pltpu.VMEM((owned, model), bf16),
+            dma((5,)),
+            dma((2,)),
+            dma((11,)),
+            dma((1,)),
             dma((3,)),
-            dma((3,)),
-            dma((units, slabs, 2)),
-            dma((units, slabs, 2)),
+            dma((1,)),
             dma((units, slabs)),
-            dma((units, slabs)),
-            dma((slabs, 4)),
-            dma((slabs, 4)),
-            dma((slabs, 4)),
-            dma((slabs, 4)),
+            dma((1,)),
+            dma((units,)),
+            dma((2,)),
+            dma((3, 4)),
+            dma((1,)),
+            dma((slabs,)),
             dma((5,)),
             dma((5,)),
-            dma((3, 2)),
-            dma((3, 2)),
-            dma((slabs, 3)),
-            dma((slabs, 3)),
+            dma((1,)),
+            dma((6,)),
+            dma((1,)),
+            dma((slabs,)),
         ],
         compiler_params=pltpu.CompilerParams(
             collective_id=0, has_side_effects=True, vmem_limit_bytes=56 * 1024 * 1024
@@ -1408,7 +1481,7 @@
         return pair_layer(
             tokens_in,
             norm_gain,
-            [w_forget, w_query, w_input, w_pool_in, w_rgate, w_pgate],
+            [w_forget, w_query, w_input, w_pool_in, w_pgate, w_rgate],
             floor_rate,
             extra_logdecay,
             state_gain,

time: 91.4 us -> 88.8 us (0.972)
  Pallas kernels: 89.3 us -> 86.5 us
    pallas_call x1, Pallas kernels: 89.3 us -> 86.5 us  [pair_layer(): pl.pallas_call(pair_kernel, out_shape=jax.ShapeDtypeStruct((owned, model)...]
where the time goes in v3:
time: 88.8 us; the launch traced here: 88.4 us
  Pallas kernels  86.5 us (97%)
  local copies, waits for them, and re-layouts  1.88 us (2%)
    pallas_call x1, Pallas kernels, pair_layer(): pl.pallas_call(pair_kernel, out_shape=jax.ShapeDtypeStruct((owned, model)...  86.5 us
    unnamed x1, local copies, waits for them, and re-layouts  1.88 us

profile of v3, /device:TPU:0, one launch (start us, length us, event | category | flops | bytes accessed | tf_op | source)
XLA Modules:
  0.0 88.4 jit_solution(14579540397612532786)
XLA Ops:
  0.0 86.5 %shard_map.154 = bf16[128,2048]{1,0:T(8,128)(2,1)} custom-call(bf16[256,1024]{1,0:T(8,128)(2,1)} %tok_hbm.1, f32[1,2048]{1,0:T(1,128)} %bitcast.6, bf16[128,512]{1,0:T(8,128)(2,1)} %w0.1, bf16[128,512]{1,0:T(8,128)(2,1)} %w1.1, bf16[128,512]{1,0:T(8,128)(2,1)} %w2.1, bf16[128,512]{1,0:T(8,128)(2,1)} %w3.1, bf16[128,512]{1,0:T(8,128)(2,1)} %w4.1, ...), custom_call_target="tpu_custom_call" | custom-call | flops 3221225472 | bytes 1572864 | tf_op jit(solution)/shard_map/pallas_call | solution.py:1382
  86.5 1.9 %copy.18 = bf16[128,2048]{1,0:T(8,128)(2,1)} copy(bf16[128,2048]{1,0:T(8,128)(2,1)} %shard_map.154) | data formatting | bytes 1048576

commit v4 on v3

--- a/solution.py
+++ b/solution.py
@@ -1014,9 +1014,11 @@
     w_relay(0, 3)
     tok_diagonal(0)
     tok_diagonal(1)
-    w_relays(1)
+    w_relay(1, 1)
     tok_diagonal(2)
+    w_relay(1, 2)
     tok_diagonal(3)
+    w_relay(1, 3)
     scale(1 - odd, c)
     tok_shared(1 - odd, False)
     scale(1 - odd, 1 - c)
@@ -1110,13 +1112,11 @@
     score_block(3)
     w_relays(4)
     o_near()
-    o_across(range(2))
+    o_across(range(pieces))
     w_need(2)
     project_units(2, 1)
     for b in range(blocks):
         value_block(b)
-        if b == 2:
-            w_relays(5)
 
     sums = [decays[2 * i + 1] * state[2 * i] + state[2 * i + 1] for i in range(2)]
     fades = [decays[2 * i] * decays[2 * i + 1] for i in range(2)]
@@ -1131,8 +1131,11 @@
         tail_go[i] = proj[3, (i + 1) * half - 16 : (i + 1) * half, :]
     send(tail_go, tail_come, scan_send.at[2], scan_recv.at[2], other_y)
     send(tail_go.at[1], last_come, scan_send.at[4], scan_recv.at[4], across_y)
+    w_relays(5)
     w_need(4)
     project_units(4, 1)
+    o_near_relays(range(2))
+    o_mid_relays(2, range(2))
 
     arrive(state_come, scan_recv.at[0])
     arrive(decay_come, scan_recv.at[1])
@@ -1152,9 +1155,6 @@
         total = fade * total + add
     total_go[...] = total.astype(bf16)
     send(total_go, total_come, scan_send.at[3], scan_recv.at[3], across)
-    o_across(range(2, pieces))
-    o_near_relays(range(2))
-    o_mid_relays(2, range(2))
     mix_copy.wait()
     arrive(tail_come, scan_recv.at[2])
     arrive(last_come, scan_recv.at[4])
@@ -1292,6 +1292,22 @@
         def _():
             over_c.start()
 
+    def drain():
+        sent(wide.at[pl.ds(0, 6 * rows // 2)], tok_send.at[1])
+        sent(extra.at[pl.ds(0, 3)], extra_send.at[0])
+        sent(w_all.at[pl.ds(0, 3), pl.ds(0, 14 * shard)], w_send.at[0])
+        sent(w_all.at[pl.ds(0, 3)], wy_send.at[0])
+        sent(o_all.at[0], o_send.at[0])
+        sent(o_all.at[pl.ds(0, 4)], oy_send.at[0])
+
+        @pl.when(is_mid)
+        def _():
+            sent(o_all.at[pl.ds(0, 4)], o_send.at[1])
+
+        for i, ref in enumerate([state_go, decay_go, tail_go, total_go, tail_go.at[1]]):
+            sent(ref, scan_send.at[i])
+        sent(y_all.at[pl.ds(0, 6)], y_send.at[0])
+
     def gather_chunk(k):
         arrive(part_come.at[k], part_recv.at[k])
         ours = part_go[k, rows_for(x, c), :].astype(f32) + part_come[k, c].astype(f32)
@@ -1311,14 +1327,13 @@
     for ch in range(2):
         o_end_relays(3, range(ch, ch + 1))
         out_chunk(2, ch)
-    for k in range(2):
-        gather_chunk(k)
-        o_end_relays(3, range(k + 2, k + 3))
-    gather_chunk(2)
+    o_end_relays(3, range(2, pieces))
     o_need(3)
     for ch in range(2):
         out_chunk(3, ch)
-    gather_chunk(3)
+    drain()
+    for k in range(len(slabs)):
+        gather_chunk(k)
 
     def finish():
         summed = mine[...]
@@ -1332,24 +1347,7 @@
         copy.wait()
 
     finish()
-    def drain():
-        sent(wide.at[pl.ds(0, 6 * rows // 2)], tok_send.at[1])
-        sent(extra.at[pl.ds(0, 3)], extra_send.at[0])
-        sent(w_all.at[pl.ds(0, 3), pl.ds(0, 14 * shard)], w_send.at[0])
-        sent(w_all.at[pl.ds(0, 3)], wy_send.at[0])
-        sent(o_all.at[0], o_send.at[0])
-        sent(o_all.at[pl.ds(0, 4)], oy_send.at[0])
-
-        @pl.when(is_mid)
-        def _():
-            sent(o_all.at[pl.ds(0, 4)], o_send.at[1])
-
-        for i, ref in enumerate([state_go, decay_go, tail_go, total_go, tail_go.at[1]]):
-            sent(ref, scan_send.at[i])
-        sent(y_all.at[pl.ds(0, 6)], y_send.at[0])
-        sent(part_go.at[pl.ds(0, 3)], part_send.at[0])
-
-    drain()
+    sent(part_go.at[pl.ds(0, 3)], part_send.at[0])
 
 
 def pair_layer(

time: 88.8 us -> 84.1 us (0.947)
  Pallas kernels: 86.5 us -> 81.9 us
    pallas_call x1, Pallas kernels: 86.5 us -> 81.9 us  [pair_layer(): pl.pallas_call(pair_kernel, out_shape=jax.ShapeDtypeStruct((owned, model)...]
where the time goes in v4:
time: 84.1 us; the launch traced here: 83.8 us
  Pallas kernels  81.9 us (97%)
  local copies, waits for them, and re-layouts  1.88 us (2%)
    pallas_call x1, Pallas kernels, pair_layer(): pl.pallas_call(pair_kernel, out_shape=jax.ShapeDtypeStruct((owned, model)...  81.9 us
    unnamed x1, local copies, waits for them, and re-layouts  1.88 us

profile of v4, /device:TPU:0, one launch (start us, length us, event | category | flops | bytes accessed | tf_op | source)
XLA Modules:
  0.0 83.8 jit_solution(9749977087893273425)
XLA Ops:
  0.0 81.9 %shard_map.154 = bf16[128,2048]{1,0:T(8,128)(2,1)} custom-call(bf16[256,1024]{1,0:T(8,128)(2,1)} %tok_hbm.1, f32[1,2048]{1,0:T(1,128)} %bitcast.6, bf16[128,512]{1,0:T(8,128)(2,1)} %w0.1, bf16[128,512]{1,0:T(8,128)(2,1)} %w1.1, bf16[128,512]{1,0:T(8,128)(2,1)} %w2.1, bf16[128,512]{1,0:T(8,128)(2,1)} %w3.1, bf16[128,512]{1,0:T(8,128)(2,1)} %w4.1, ...), custom_call_target="tpu_custom_call" | custom-call | flops 3221225472 | bytes 1572864 | tf_op jit(solution)/shard_map/pallas_call | solution.py:1380
  81.9 1.9 %copy.18 = bf16[128,2048]{1,0:T(8,128)(2,1)} copy(bf16[128,2048]{1,0:T(8,128)(2,1)} %shard_map.154) | data formatting | bytes 1048576

commit v5 on v4

--- a/solution.py
+++ b/solution.py
@@ -840,6 +840,8 @@
             src_ref=src, dst_ref=dst, send_sem=send_sem, recv_sem=recv_sem, device_id=to
         )
 
+    ahead = 1
+
     def w_send_to(u, k, only=None):
         copies = []
         for e in range(2):
@@ -881,6 +883,8 @@
         )
         w_send_to(u, 1, None if u == 0 else is_mid)
         w_send_to(u, 2, is_mid)
+        if u < ahead:
+            w_send_to(u, 3, is_mid)
 
     def w_relay(u, k):
         at = w_all.at[u, w_piece(slabs[k], 0, 2)]
@@ -895,7 +899,7 @@
                 w_send_to(u, 1, is_end)
 
     def w_late_mid():
-        for u in range(units):
+        for u in range(ahead, units):
             w_send_to(u, 3, is_mid)
 
     def w_need(u):
@@ -1014,8 +1018,8 @@
     w_relay(0, 3)
     tok_diagonal(0)
     tok_diagonal(1)
+    tok_diagonal(2)
     w_relay(1, 1)
-    tok_diagonal(2)
     w_relay(1, 2)
     tok_diagonal(3)
     w_relay(1, 3)
@@ -1252,7 +1256,6 @@
     o_end_relays(2, range(2))
     y_pass(0, 0)
     o_mid_relays(3, range(2, pieces))
-    o_end_relays(2, range(2, pieces))
     y_pass(0, 1)
 
     owned = part_come.shape[2]
@@ -1260,32 +1263,37 @@
     def rows_for(xx, cc):
         return own_rows(cc * rows + xx * owned, owned)
 
-    def part_copies(k, ch):
+    def part_copies(k, ch, cols):
         over_x = send_copy(
-            part_go.at[k, rows_for(1 - x, ch)],
-            part_come.at[k, c],
+            part_go.at[k, rows_for(1 - x, ch), cols],
+            part_come.at[k, c, :, cols],
             part_send.at[0],
             part_recv.at[k],
             peer_x(ch),
         )
         over_c = send_copy(
-            part_go.at[k, rows_for(x, ch)],
-            part_come.at[k, 2],
+            part_go.at[k, rows_for(x, ch), cols],
+            part_come.at[k, 2, :, cols],
             part_send.at[0],
             part_recv.at[k],
             other_c,
         )
         return over_x, over_c
 
-    def out_chunk(k, ch):
+    def out_chunk(k, ch, yy=None):
         left = jnp.concatenate(
             [y_all[i, ch * block : (ch + 1) * block, :] for i in range(8)], axis=1
         )
-        right = jnp.concatenate([o_all[slabs[k] * 2], o_all[slabs[k] * 2 + 1]], axis=1)
-        part_go[k, ch * block : (ch + 1) * block, :] = jnp.dot(
+        if yy is None:
+            right = jnp.concatenate([o_all[slabs[k] * 2], o_all[slabs[k] * 2 + 1]], axis=1)
+            cols = pl.ds(0, 2 * DK)
+        else:
+            right = o_all[slabs[k] * 2 + yy]
+            cols = lanes(yy)
+        part_go[k, ch * block : (ch + 1) * block, cols] = jnp.dot(
             left, right, preferred_element_type=f32
         ).astype(bf16)
-        over_x, over_c = part_copies(k, ch)
+        over_x, over_c = part_copies(k, ch, cols)
         over_x.start()
 
         @pl.when(c != ch)
@@ -1317,20 +1325,28 @@
             mine[:, lanes(slabs[k] * 4 + yy * 2 + c)] = ours[:, cols]
             mine[:, lanes(slabs[k] * 4 + yy * 2 + 1 - c)] = others[:, cols]
 
+    late = [(2, 2), (2, 3), (3, 0), (3, 1), (3, 2), (3, 3)]
+
+    def late_relay():
+        k, part = late.pop(0)
+        o_end_relays(k, [part])
+
     for ch in range(2):
         y_need(ch)
         for k in range(2):
             if ch == 0:
                 o_need(k)
             out_chunk(k, ch)
+            late_relay()
     o_need(2)
     for ch in range(2):
-        o_end_relays(3, range(ch, ch + 1))
         out_chunk(2, ch)
-    o_end_relays(3, range(2, pieces))
+        late_relay()
+    for ch in range(2):
+        out_chunk(3, ch, y)
     o_need(3)
     for ch in range(2):
-        out_chunk(3, ch)
+        out_chunk(3, ch, 1 - y)
     drain()
     for k in range(len(slabs)):
         gather_chunk(k)

time: 84.1 us -> 80.6 us (0.958)
  Pallas kernels: 81.9 us -> 78.5 us
    pallas_call x1, Pallas kernels: 81.9 us -> 78.5 us  [pair_layer(): pl.pallas_call(pair_kernel, out_shape=jax.ShapeDtypeStruct((owned, model)...]
where the time goes in v5:
time: 80.6 us; the launch traced here: 80.4 us
  Pallas kernels  78.5 us (97%)
  local copies, waits for them, and re-layouts  1.88 us (2%)
    pallas_call x1, Pallas kernels, pair_layer(): pl.pallas_call(pair_kernel, out_shape=jax.ShapeDtypeStruct((owned, model)...  78.5 us
    unnamed x1, local copies, waits for them, and re-layouts  1.88 us

profile of v5, /device:TPU:0, one launch (start us, length us, event | category | flops | bytes accessed | tf_op | source)
XLA Modules:
  0.0 80.4 jit_solution(9069191488192502400)
XLA Ops:
  0.0 78.5 %shard_map.154 = bf16[128,2048]{1,0:T(8,128)(2,1)} custom-call(bf16[256,1024]{1,0:T(8,128)(2,1)} %tok_hbm.1, f32[1,2048]{1,0:T(1,128)} %bitcast.6, bf16[128,512]{1,0:T(8,128)(2,1)} %w0.1, bf16[128,512]{1,0:T(8,128)(2,1)} %w1.1, bf16[128,512]{1,0:T(8,128)(2,1)} %w2.1, bf16[128,512]{1,0:T(8,128)(2,1)} %w3.1, bf16[128,512]{1,0:T(8,128)(2,1)} %w4.1, ...), custom_call_target="tpu_custom_call" | custom-call | flops 3221225472 | bytes 1572864 | tf_op jit(solution)/shard_map/pallas_call | solution.py:1396
  78.5 1.9 %copy.18 = bf16[128,2048]{1,0:T(8,128)(2,1)} copy(bf16[128,2048]{1,0:T(8,128)(2,1)} %shard_map.154) | data formatting | bytes 1048576

commit v6 on v5

--- a/solution.py
+++ b/solution.py
@@ -659,21 +659,21 @@
 
 def pair_kernel(
     tok_hbm,
-    gain_ref,
+    gain_hbm,
     w0,
     w1,
     w2,
     w3,
     w4,
     w5,
-    rate_ref,
+    rate_hbm,
     extra_hbm,
-    sgain_ref,
+    sgain_hbm,
     mix_hbm,
-    pgain_ref,
+    pgain_hbm,
     orec_hbm,
     opool_hbm,
-    post_ref,
+    post_hbm,
     out_ref,
     wide,
     scaled,
@@ -705,6 +705,12 @@
     part_come,
     mine,
     done,
+    gain_ref,
+    rate_ref,
+    sgain_ref,
+    pgain_ref,
+    post_ref,
+    small_sem,
     own_sem,
     tok_send,
     tok_recv,
@@ -767,6 +773,15 @@
         start = zq * half + cc * rows + q * piece
         return wide.at[own_rows(start, piece), pl.ds(pl.multiple_of(xx * feats, 128), feats)]
 
+    barrier = pltpu.get_barrier_semaphore()
+    across = peer((z + 2) % 4, y, c)
+    across_y = peer((z + 2) % 4, 1 - y, c)
+    peers = [other_c, other_y, peer_x(c), peer_x(1 - c), across_y]
+    for k in range(1, 4):
+        peers += [peer(slabs[k], y, c), peer(slabs[k], y, 1 - c)]
+    for to in peers:
+        pl.semaphore_signal(barrier, inc=1, device_id=to)
+
     owns = {}
 
     def own_copy(name, src, dst):
@@ -788,15 +803,19 @@
     pltpu.make_async_copy(opool_hbm, o_all.at[here, pl.ds(4 * DK, 4 * DK)], o_landed).start()
     mix_copy = pltpu.make_async_copy(mix_hbm.at[head], mix_own, own_sem.at[4])
     mix_copy.start()
-
-    barrier = pltpu.get_barrier_semaphore()
-    across = peer((z + 2) % 4, y, c)
-    across_y = peer((z + 2) % 4, 1 - y, c)
-    peers = [other_c, other_y, peer_x(c), peer_x(1 - c), across_y]
-    for k in range(1, 4):
-        peers += [peer(slabs[k], y, c), peer(slabs[k], y, 1 - c)]
-    for to in peers:
-        pl.semaphore_signal(barrier, inc=1, device_id=to)
+    smalls = []
+    for i, (src, dst) in enumerate(
+        [
+            (gain_hbm, gain_ref),
+            (rate_hbm, rate_ref),
+            (sgain_hbm, sgain_ref),
+            (pgain_hbm, pgain_ref),
+            (post_hbm, post_ref),
+        ]
+    ):
+        smalls.append(pltpu.make_async_copy(src, dst, small_sem.at[i]))
+        smalls[-1].start()
+
     pl.semaphore_wait(barrier, len(peers))
 
     def send(src, dst, send_sem, recv_sem, to):
@@ -931,7 +950,8 @@
         at = o_at(slabs[k], y, part)
         if k > 0:
             arrive(at, o_recv.at[k - 1, part])
-        send(at, at, oy_send.at[0], oy_recv.at[k], other_y)
+        slot = 4 if (k, part) == (3, pieces - 1) else k
+        send(at, at, oy_send.at[0], oy_recv.at[slot], other_y)
 
     def o_onward(k, part):
         if k == 1:
@@ -962,6 +982,12 @@
 
     def o_need(k):
         arrive(o_all.at[slabs[k] * 2 + 1 - y], oy_recv.at[k])
+
+    def o_need_most():
+        arrive(o_all.at[slabs[3] * 2 + 1 - y, pl.ds(0, (pieces - 1) * depth)], oy_recv.at[3])
+
+    def o_need_last():
+        arrive(o_at(slabs[3], 1 - y, pieces - 1), oy_recv.at[4])
 
     for u in range(units):
         w_relay(u, 0)
@@ -1010,6 +1036,8 @@
     w_late_mid()
     tok_z(3)
     tok_x()
+    for copy in smalls:
+        copy.wait()
     scale(odd, c)
     tok_shared(odd, True)
     scale(odd, 1 - c)
@@ -1037,6 +1065,24 @@
             norm = inv_rms[at, :]
             for j in range(count):
                 proj[first + j, at, :] = (acc[:, j * DK : (j + 1) * DK] * norm).astype(bf16)
+            return 0
+
+        lax.fori_loop(0, blocks, one, 0)
+
+    def project_side(u, yy, last):
+        def one(i, _):
+            at = own_rows(i * block, block)
+            acc = kept[0, at, :] if last else jnp.zeros((block, DK), f32)
+            for slab in range(len(slabs)):
+                start = pl.multiple_of((slab * 4 + yy * 2) * shard, 2 * shard)
+                deep = pl.ds(start, 2 * shard)
+                acc = acc + jnp.dot(
+                    scaled[at, deep], w_all[u, deep, :], preferred_element_type=f32
+                )
+            if last:
+                proj[u, at, :] = (acc * inv_rms[at, :]).astype(bf16)
+            else:
+                kept[0, at, :] = acc
             return 0
 
         lax.fori_loop(0, blocks, one, 0)
@@ -1128,18 +1174,18 @@
         state_go[i] = sums[i].astype(bf16)
         decay_go[i : i + 1, :] = fades[i]
     send(state_go, state_come, scan_send.at[0], scan_recv.at[0], other_y)
-    send(decay_go, decay_come, scan_send.at[1], scan_recv.at[1], other_y)
+    send(decay_go, decay_come, scan_send.at[0], scan_recv.at[1], other_y)
     w_need(3)
     project_units(3, 1)
     for i in range(2):
         tail_go[i] = proj[3, (i + 1) * half - 16 : (i + 1) * half, :]
-    send(tail_go, tail_come, scan_send.at[2], scan_recv.at[2], other_y)
-    send(tail_go.at[1], last_come, scan_send.at[4], scan_recv.at[4], across_y)
+    send(tail_go, tail_come, scan_send.at[0], scan_recv.at[2], other_y)
+
+    @pl.when(pair == 0)
+    def _():
+        send(tail_go.at[1], last_come, scan_send.at[1], scan_recv.at[4], across_y)
+
     w_relays(5)
-    w_need(4)
-    project_units(4, 1)
-    o_near_relays(range(2))
-    o_mid_relays(2, range(2))
 
     arrive(state_come, scan_recv.at[0])
     arrive(decay_come, scan_recv.at[1])
@@ -1158,19 +1204,34 @@
     for add, fade in order[1:]:
         total = fade * total + add
     total_go[...] = total.astype(bf16)
-    send(total_go, total_come, scan_send.at[3], scan_recv.at[3], across)
+
+    @pl.when(pair == 0)
+    def _():
+        send(total_go, total_come, scan_send.at[1], scan_recv.at[3], across)
+
+    w_need(4)
+    project_units(4, 1)
+    o_near_relays(range(2))
+    o_mid_relays(2, range(2))
     mix_copy.wait()
     arrive(tail_come, scan_recv.at[2])
-    arrive(last_come, scan_recv.at[4])
-
-    later_pair = pair > 0
+
+    @pl.when(pair > 0)
+    def _():
+        arrive(last_come, scan_recv.at[4])
+
+    @pl.when(pair == 0)
+    def _():
+        last_come[...] = jnp.zeros_like(last_come)
+
+
     at_head = lanes(head)
     level = (x * 4 + head) % 4
     window = 2
     for k in range(1, 4):
         window = jnp.where(level == k, 2 ** (1 + k), window)
     line_half = lax.broadcasted_iota(jnp.int32, (half, DK), 0)
-    far = [jnp.where(later_pair, last_come[...].astype(f32), 0.0), tail_come[0].astype(f32)]
+    far = [last_come[...].astype(f32), tail_come[0].astype(f32)]
     their_tails = [tail_come[i].astype(f32) for i in range(2)]
     is_odd = odd == 1
 
@@ -1223,11 +1284,20 @@
         rows_ch = slice(ch * block, (ch + 1) * block)
         y_put(1, ch, pooled[0][rows_ch], pooled[1][rows_ch])
     o_near_relays(range(2, pieces))
+    project_side(5, y, False)
     w_need(5)
-    project_units(5, 1)
-    arrive(total_come, scan_recv.at[3])
+    project_side(5, 1 - y, True)
+
+    @pl.when(pair > 0)
+    def _():
+        arrive(total_come, scan_recv.at[3])
+
+    @pl.when(pair == 0)
+    def _():
+        total_come[...] = jnp.zeros_like(total_come)
+
     befores = []
-    running = jnp.where(later_pair, total_come[...].astype(f32), 0.0)
+    running = total_come[...].astype(f32)
     for i in range(2):
         after_first = order[2 * i][1] * running + order[2 * i][0]
         befores.append(jnp.where(first_y, running, after_first))
@@ -1280,19 +1350,23 @@
         )
         return over_x, over_c
 
-    def out_chunk(k, ch, yy=None):
+    def out_chunk(k, ch, yy=None, rest=False):
+        at = slice(ch * block, (ch + 1) * block)
         left = jnp.concatenate(
-            [y_all[i, ch * block : (ch + 1) * block, :] for i in range(8)], axis=1
+            [y_all[i, at, :] for i in range(6 if rest else 0, 8)], axis=1
         )
         if yy is None:
             right = jnp.concatenate([o_all[slabs[k] * 2], o_all[slabs[k] * 2 + 1]], axis=1)
             cols = pl.ds(0, 2 * DK)
         else:
             right = o_all[slabs[k] * 2 + yy]
+            if rest:
+                right = o_all[slabs[k] * 2 + yy, pl.ds((pieces - 1) * depth, depth), :]
             cols = lanes(yy)
-        part_go[k, ch * block : (ch + 1) * block, cols] = jnp.dot(
-            left, right, preferred_element_type=f32
-        ).astype(bf16)
+        value = jnp.dot(left, right, preferred_element_type=f32)
+        if rest:
+            value = value + kept[1, at, :]
+        part_go[k, at, cols] = value.astype(bf16)
         over_x, over_c = part_copies(k, ch, cols)
         over_x.start()
 
@@ -1312,8 +1386,12 @@
         def _():
             sent(o_all.at[pl.ds(0, 4)], o_send.at[1])
 
-        for i, ref in enumerate([state_go, decay_go, tail_go, total_go, tail_go.at[1]]):
-            sent(ref, scan_send.at[i])
+        sent(w_all.at[0, pl.ds(0, 2 * DK + 3 * DK // 8)], scan_send.at[0])
+
+        @pl.when(pair == 0)
+        def _():
+            sent(w_all.at[0, pl.ds(0, DK + DK // 8)], scan_send.at[1])
+
         sent(y_all.at[pl.ds(0, 6)], y_send.at[0])
 
     def gather_chunk(k):
@@ -1344,23 +1422,26 @@
         late_relay()
     for ch in range(2):
         out_chunk(3, ch, y)
-    o_need(3)
+    o_need_most()
     for ch in range(2):
-        out_chunk(3, ch, 1 - y)
+        at = slice(ch * block, (ch + 1) * block)
+        left = jnp.concatenate([y_all[i, at, :] for i in range(6)], axis=1)
+        right = o_all[slabs[3] * 2 + 1 - y, pl.ds(0, (pieces - 1) * depth), :]
+        kept[1, at, :] = jnp.dot(left, right, preferred_element_type=f32)
+    o_need_last()
+    for ch in range(2):
+        out_chunk(3, ch, 1 - y, True)
     drain()
     for k in range(len(slabs)):
         gather_chunk(k)
 
     def finish():
         summed = mine[...]
-        done[...] = (
+        out_ref[...] = (
             summed
             * lax.rsqrt(jnp.mean(summed * summed, axis=1, keepdims=True) + eps)
             * post_ref[...]
         ).astype(bf16)
-        copy = pltpu.make_async_copy(done, out_ref, own_sem.at[0])
-        copy.start()
-        copy.wait()
 
     finish()
     sent(part_go.at[pl.ds(0, 3)], part_send.at[0])
@@ -1392,12 +1473,12 @@
     model = n * width
     f32, bf16, dma = jnp.float32, jnp.bfloat16, pltpu.SemaphoreType.DMA
     units = len(shards)
-    vmem, hbm = pl.BlockSpec(memory_space=pltpu.VMEM), pl.BlockSpec(memory_space=pl.ANY)
+    hbm = pl.BlockSpec(memory_space=pl.ANY)
     return pl.pallas_call(
         pair_kernel,
-        out_shape=jax.ShapeDtypeStruct((owned, model), bf16),
-        in_specs=[hbm, vmem] + [hbm] * 6 + [vmem, hbm, vmem, hbm, vmem, hbm, hbm, vmem],
-        out_specs=hbm,
+        out_shape=pltpu.VMEM((owned, model), bf16),
+        in_specs=[pl.BlockSpec(memory_space=pltpu.HBM)] * 16,
+        out_specs=pl.BlockSpec(memory_space=pltpu.VMEM),
         scratch_shapes=[
             pltpu.VMEM((positions, n_tp * feats), bf16),
             pltpu.VMEM((positions, n_tp * feats), bf16),
@@ -1429,6 +1510,12 @@
             pltpu.VMEM((slabs, 3, owned, 2 * width), bf16),
             pltpu.VMEM((owned, model), f32),
             pltpu.VMEM((owned, model), bf16),
+            pltpu.VMEM((1, n_tp * feats), f32),
+            pltpu.VMEM((1, cols), f32),
+            pltpu.VMEM((1, cols), f32),
+            pltpu.VMEM((1, cols), f32),
+            pltpu.VMEM((1, model), f32),
+            dma((5,)),
             dma((5,)),
             dma((2,)),
             dma((11,)),
@@ -1441,8 +1528,8 @@
             dma((2,)),
             dma((3, 4)),
             dma((1,)),
-            dma((slabs,)),
-            dma((5,)),
+            dma((slabs + 1,)),
+            dma((2,)),
             dma((5,)),
             dma((1,)),
             dma((6,)),
@@ -1450,7 +1537,7 @@
             dma((slabs,)),
         ],
         compiler_params=pltpu.CompilerParams(
-            collective_id=0, has_side_effects=True, vmem_limit_bytes=56 * 1024 * 1024
+            collective_id=0, has_side_effects=True, vmem_limit_bytes=32 * 1024 * 1024
         ),
         cost_estimate=pl.CostEstimate(
             flops=2 * positions * n * shard * units * DK,
@@ -1458,17 +1545,22 @@
             transcendentals=0,
         ),
     )(
-        tokens,
-        gain[None, :],
-        *shards,
-        rate[None, :],
-        extra.T,
-        sgain[None, :],
-        pool_mix,
-        pgain[None, :],
-        out_rec,
-        out_pool,
-        post[None, :],
+        *(
+            pltpu.with_memory_space_constraint(value, pltpu.HBM)
+            for value in (
+                tokens,
+                gain[None, :],
+                *shards,
+                rate[None, :],
+                extra.T,
+                sgain[None, :],
+                pool_mix,
+                pgain[None, :],
+                out_rec,
+                out_pool,
+                post[None, :],
+            )
+        )
     )
 
 

time: 80.6 us -> 78 us (0.968)
  Pallas kernels: 78.5 us -> 77 us
  local copies, waits for them, and re-layouts: 1.88 us -> 0.8 us
    pallas_call x1, Pallas kernels: 78.5 us -> 77 us  [pair_layer(): pl.pallas_call(pair_kernel, out_shape=pltpu.VMEM((owned, model), bf16), i...]
    unnamed x1, local copies, waits for them, and re-layouts: 1.88 us -> 0.8 us
where the time goes in v6:
time: 78 us; the launch traced here: 77.8 us
  Pallas kernels  77 us (99%)
  local copies, waits for them, and re-layouts  0.8 us (1%)
    pallas_call x1, Pallas kernels, pair_layer(): pl.pallas_call(pair_kernel, out_shape=pltpu.VMEM((owned, model), bf16), i...  77 us

profile of v6, /device:TPU:0, one launch (start us, length us, event | category | flops | bytes accessed | tf_op | source)
XLA Modules:
  0.0 77.8 jit_solution(10586917769705339514)
XLA Ops:
  0.0 77.0 %shard_map.154 = bf16[128,2048]{1,0:T(8,128)(2,1)S(1)} custom-call(bf16[256,1024]{1,0:T(8,128)(2,1)} %tok_hbm.1, f32[1,2048]{1,0:T(1,128)} %bitcast.6, bf16[128,512]{1,0:T(8,128)(2,1)} %w0.1, bf16[128,512]{1,0:T(8,128)(2,1)} %w1.1, bf16[128,512]{1,0:T(8,128)(2,1)} %w2.1, bf16[128,512]{1,0:T(8,128)(2,1)} %w3.1, bf16[128,512]{1,0:T(8,128)(2,1)} %w4.1, ...), custom_call_target="tpu_custom_call" | custom-call | flops 3221225472 | bytes 1572864 | tf_op jit(solution)/shard_map/pallas_call | solution.py:1477
  77.0 0.8 %copy.18 = bf16[128,2048]{1,0:T(8,128)(2,1)} copy(bf16[128,2048]{1,0:T(8,128)(2,1)S(1)} %shard_map.154) | data formatting | bytes 1048576

commit v7 on v6

--- a/solution.py
+++ b/solution.py
@@ -924,7 +924,7 @@
     def w_need(u):
         arrive(w_all.at[u, pl.ds(0, n_rows // 2)], wy_recv.at[u])
 
-    pieces = 4
+    pieces = 8
     depth = o_all.shape[1] // pieces
 
     def o_at(slab, yy, part):
@@ -1211,8 +1211,8 @@
 
     w_need(4)
     project_units(4, 1)
-    o_near_relays(range(2))
-    o_mid_relays(2, range(2))
+    o_near_relays(range(4))
+    o_mid_relays(2, range(4))
     mix_copy.wait()
     arrive(tail_come, scan_recv.at[2])
 
@@ -1283,10 +1283,8 @@
     for ch in range(2):
         rows_ch = slice(ch * block, (ch + 1) * block)
         y_put(1, ch, pooled[0][rows_ch], pooled[1][rows_ch])
-    o_near_relays(range(2, pieces))
+    o_near_relays(range(4, pieces))
     project_side(5, y, False)
-    w_need(5)
-    project_side(5, 1 - y, True)
 
     @pl.when(pair > 0)
     def _():
@@ -1309,23 +1307,31 @@
             reach[rows_b, :], before.astype(bf16), over_last, preferred_element_type=f32
         )
         normed = rec * lax.rsqrt(jnp.mean(rec * rec, axis=1, keepdims=True) + eps)
-        gate = proj[5, rows_b, :].astype(f32)
-        return normed * sgain_ref[:, at_head] * (gate * jax.nn.sigmoid(gate))
+        local[rows_b, :] = normed * sgain_ref[:, at_head]
 
     for ch in range(2):
-        recs = []
         for i in range(2):
             b = 2 * i + ch
-            recs.append(rec_rows(b, befores[i]))
+            rec_rows(b, befores[i])
             befores[i] = decays[b] * befores[i] + state[b]
+
+    def gated(b):
+        rows_b = slice(b * block, (b + 1) * block)
+        gate = proj[5, rows_b, :].astype(f32)
+        return local[rows_b, :] * (gate * jax.nn.sigmoid(gate))
+
+    w_need(5)
+    project_side(5, 1 - y, True)
+    for ch in range(2):
+        recs = [gated(2 * i + ch) for i in range(2)]
         y_put(0, ch, recs[0], recs[1])
-    o_mid_relays(2, range(2, pieces))
+    o_mid_relays(2, range(4, pieces))
     for ch in range(2):
         y_pass(1, ch)
-    o_mid_relays(3, range(2))
-    o_end_relays(2, range(2))
+    o_mid_relays(3, range(4))
+    o_end_relays(2, range(4))
     y_pass(0, 0)
-    o_mid_relays(3, range(2, pieces))
+    o_mid_relays(3, range(4, pieces))
     y_pass(0, 1)
 
     owned = part_come.shape[2]
@@ -1353,7 +1359,7 @@
     def out_chunk(k, ch, yy=None, rest=False):
         at = slice(ch * block, (ch + 1) * block)
         left = jnp.concatenate(
-            [y_all[i, at, :] for i in range(6 if rest else 0, 8)], axis=1
+            [y_all[i, at, :] for i in range(7 if rest else 0, 8)], axis=1
         )
         if yy is None:
             right = jnp.concatenate([o_all[slabs[k] * 2], o_all[slabs[k] * 2 + 1]], axis=1)
@@ -1403,11 +1409,11 @@
             mine[:, lanes(slabs[k] * 4 + yy * 2 + c)] = ours[:, cols]
             mine[:, lanes(slabs[k] * 4 + yy * 2 + 1 - c)] = others[:, cols]
 
-    late = [(2, 2), (2, 3), (3, 0), (3, 1), (3, 2), (3, 3)]
+    late = [(2, 4), (2, 6), (3, 0), (3, 2), (3, 4), (3, 6)]
 
     def late_relay():
         k, part = late.pop(0)
-        o_end_relays(k, [part])
+        o_end_relays(k, [part, part + 1])
 
     for ch in range(2):
         y_need(ch)
@@ -1425,7 +1431,7 @@
     o_need_most()
     for ch in range(2):
         at = slice(ch * block, (ch + 1) * block)
-        left = jnp.concatenate([y_all[i, at, :] for i in range(6)], axis=1)
+        left = jnp.concatenate([y_all[i, at, :] for i in range(7)], axis=1)
         right = o_all[slabs[3] * 2 + 1 - y, pl.ds(0, (pieces - 1) * depth), :]
         kept[1, at, :] = jnp.dot(left, right, preferred_element_type=f32)
     o_need_last()
@@ -1526,7 +1532,7 @@
             dma((1,)),
             dma((units,)),
             dma((2,)),
-            dma((3, 4)),
+            dma((3, 8)),
             dma((1,)),
             dma((slabs + 1,)),
             dma((2,)),

time: 78 us -> 78.4 us (level)
  no operation moved by 1% of the time
where the time goes in v7:
time: 78.4 us; the launch traced here: 78.2 us
  Pallas kernels  77.4 us (99%)
  local copies, waits for them, and re-layouts  0.8 us (1%)
    pallas_call x1, Pallas kernels, pair_layer(): pl.pallas_call(pair_kernel, out_shape=pltpu.VMEM((owned, model), bf16), i...  77.4 us

profile of v7, /device:TPU:0, one launch (start us, length us, event | category | flops | bytes accessed | tf_op | source)
XLA Modules:
  0.0 78.2 jit_solution(9022903917798252118)
XLA Ops:
  0.0 77.4 %shard_map.154 = bf16[128,2048]{1,0:T(8,128)(2,1)S(1)} custom-call(bf16[256,1024]{1,0:T(8,128)(2,1)} %tok_hbm.1, f32[1,2048]{1,0:T(1,128)} %bitcast.6, bf16[128,512]{1,0:T(8,128)(2,1)} %w0.1, bf16[128,512]{1,0:T(8,128)(2,1)} %w1.1, bf16[128,512]{1,0:T(8,128)(2,1)} %w2.1, bf16[128,512]{1,0:T(8,128)(2,1)} %w3.1, bf16[128,512]{1,0:T(8,128)(2,1)} %w4.1, ...), custom_call_target="tpu_custom_call" | custom-call | flops 3221225472 | bytes 1572864 | tf_op jit(solution)/shard_map/pallas_call | solution.py:1483
  77.5 0.8 %copy.18 = bf16[128,2048]{1,0:T(8,128)(2,1)} copy(bf16[128,2048]{1,0:T(8,128)(2,1)S(1)} %shard_map.154) | data formatting | bytes 1048576
